TPU v7x, 256 devices: a whole 4x4x8 slice. The times are simulated.
256 devices in a mesh: sp: 32 (over z, x), tp: 8 (over y, core).
Axes of the slice: x: 4, y: 4, z: 8, core: 2. Of those that a mesh axis runs over, the one named last changes fastest.
Arguments:
- queries: bfloat16 [16384, 1024], P('sp', 'tp'), may hold values from -5.5 to 5.5
- key_vectors: bfloat16 [16384, 1024], P('sp', 'tp'), may hold values from -5.5 to 5.5
- latents: bfloat16 [16384, 2048], P('sp', 'tp'), may hold values from -6 to 6
- w_value: bfloat16 [2048, 1024], P(None, 'tp'), may hold values from -0.125 to 0.125
- log_sums: float32 [16384, 16], P('sp', 'tp'), as said below
- out_pair: bfloat16 [16384, 2048], P('sp', 'tp'), may hold values from -6 to 6
- cotangent: bfloat16 [16384, 1024], P('sp', 'tp'), may hold values from -6 to 6
- lambdas: float32 [8], P('tp'), may hold values from 0.3 to 0.8
- out_gain: float32 [128], replicated, may hold values from 0.1 to 1.9
Outputs:
- query_grad: float32 [16384, 1024], P('sp', 'tp')
- key_grad: float32 [16384, 1024], P('sp', 'tp')
- value_grad: float32 [16384, 1024], P('sp', 'tp')
- weight_grad: float32 [2048, 1024], P('sp', 'tp')
Inputs may be any that keep to these rules, and one draw needn't show every extreme that they name: `log_sums`: each entry is the logarithm of the sum of exp(scores_c[t, s]) over s <= t for its row t, head h and map c.
All inputs are finite; a program needn't handle non-finite values.
Results may differ from a plain program's by a relative error of at most 0.008.
Values may be sent and summed in bfloat16 or wider, within the bound.
A program may use at most 64 MiB of HBM per device.

v0:
```python
import jax
import jax.numpy as jnp
from jax import lax
from jax.sharding import PartitionSpec as P

norm_floor = 0.25
block_rows = 512


def sent_to_all(x, axis):
    copies = jnp.broadcast_to(x, (lax.axis_size(axis), *x.shape))
    return lax.all_to_all(copies, axis, split_axis=0, concat_axis=0, tiled=True)


def laid_out(pieces, dim):
    lengths = list(pieces.shape[1:])
    lengths[dim] *= pieces.shape[0]
    return jnp.moveaxis(pieces, 0, dim).reshape(lengths)


def gathered_copies(x, axis, dim):
    pieces = sent_to_all(x, axis)
    return laid_out(pieces, dim)


def cut_along(x, dim, devices):
    lengths = x.shape
    pieces = x.reshape(*lengths[:dim], devices, lengths[dim] // devices, *lengths[dim + 1 :])
    return jnp.moveaxis(pieces, dim, 0)


def sent_and_summed(x, axis, dim):
    pieces = cut_along(x, dim, lax.axis_size(axis))
    arrived = lax.all_to_all(pieces, axis, split_axis=0, concat_axis=0, tiled=True)
    return arrived.sum(axis=0)


def head_cotangent(out_pair, cotangent, lambdas, out_gain):
    tok_rows = out_pair.shape[0]
    head_count = lambdas.shape[0]
    out_maps = out_pair.astype(jnp.float32).reshape(tok_rows, head_count, 2, -1)
    lam_cols = lambdas[None, :, None]
    merged = out_maps[:, :, 0] - lam_cols * out_maps[:, :, 1]
    inv_norm = lax.rsqrt(jnp.mean(merged * merged, axis=-1, keepdims=True) + norm_floor)
    scaled = cotangent.astype(jnp.float32).reshape(merged.shape) * out_gain
    inner_dot = jnp.mean(scaled * merged, axis=-1, keepdims=True)
    out_grad = (inv_norm * scaled - merged * (inv_norm * inv_norm * inv_norm) * inner_dot).astype(
        jnp.bfloat16
    )
    grad_wide = out_grad.astype(jnp.float32)
    first_map = jnp.sum(grad_wide * out_maps[:, :, 0], axis=-1)
    second_map = -lambdas[None, :] * jnp.sum(grad_wide * out_maps[:, :, 1], axis=-1)
    return (out_grad, jnp.stack([first_map, second_map], axis=-1))


def block_terms(
    query_block,
    key_block,
    value_block,
    grad_block,
    log_block,
    term_block,
    lambdas,
    query_pos,
    key_pos,
):
    factor = query_block.shape[-1] ** (-0.5)
    scores = (
        jnp.einsum("qhcd,khcd->hcqk", query_block, key_block, preferred_element_type=jnp.float32)
        * factor
    )
    visible = key_pos[None, :] <= query_pos[:, None]
    shifted = scores - jnp.transpose(log_block, (1, 2, 0))[..., None]
    softmax_maps = jnp.where(visible, jnp.exp(shifted), 0.0)
    value_dot = jnp.einsum(
        "qhe,khe->hqk", grad_block, value_block, preferred_element_type=jnp.float32
    )
    lam_cols = lambdas[:, None, None]
    weights = (softmax_maps[:, 0] - lam_cols * softmax_maps[:, 1]).astype(jnp.bfloat16)
    term_cols = jnp.transpose(term_block, (1, 2, 0))
    first_map = softmax_maps[:, 0] * (value_dot - term_cols[:, 0, :, None])
    second_map = softmax_maps[:, 1] * (-lam_cols * value_dot - term_cols[:, 1, :, None])
    dscore = (jnp.stack([first_map, second_map], axis=1) * factor).astype(jnp.bfloat16)
    return (weights, dscore)


def block_span():
    return block_rows


def per_device(
    queries, key_vectors, latents, w_value, log_sums, out_pair, cotangent, lambdas, out_gain
):
    tok_rows = queries.shape[0]
    head_count = lambdas.shape[0]
    offset = lax.axis_index("sp") * tok_rows
    own_pos = offset + jnp.arange(tok_rows, dtype=jnp.int32)
    last_pos = offset + tok_rows - 1
    gathered = gathered_copies(latents, "tp", 1)
    values = jnp.dot(gathered, w_value, preferred_element_type=jnp.float32).astype(jnp.bfloat16)
    out_grad, row_terms = head_cotangent(out_pair, cotangent, lambdas, out_gain)
    query_heads = queries.reshape(tok_rows, head_count, 2, -1)
    key_heads = key_vectors.reshape(tok_rows, head_count, 2, -1)
    value_heads = values.reshape(tok_rows, head_count, -1)
    log_heads = log_sums.reshape(tok_rows, head_count, 2)
    grad_flat = out_grad.reshape(tok_rows, -1)
    term_flat = row_terms.reshape(tok_rows, -1)
    zero_keys = jnp.zeros(key_heads.shape, jnp.float32)
    zero_values = jnp.zeros(value_heads.shape, jnp.float32)
    partial_value = (zero_keys, zero_keys, zero_values)
    running = partial_value[0]
    key_piece = lax.all_gather(key_vectors.astype(jnp.float32), "sp", axis=0, tiled=True).astype(
        jnp.bfloat16
    )
    value_piece = lax.all_gather(values.astype(jnp.float32), "sp", axis=0, tiled=True).astype(
        jnp.bfloat16
    )
    piece_rows = key_piece.shape[0]
    block_len = block_span()

    def query_add_block(block_idx, partial_value):
        begin_row = block_idx * block_len
        key_block = lax.dynamic_slice_in_dim(key_piece, begin_row, block_len, 0).reshape(
            block_len, head_count, 2, -1
        )
        value_block = lax.dynamic_slice_in_dim(value_piece, begin_row, block_len, 0).reshape(
            block_len, head_count, -1
        )
        key_pos = begin_row + jnp.arange(block_len, dtype=jnp.int32)

        def query_compute(sums):
            weights, dscore = block_terms(
                query_heads,
                key_block,
                value_block,
                out_grad,
                log_heads,
                row_terms,
                lambdas,
                own_pos,
                key_pos,
            )
            return sums + jnp.einsum(
                "hcqk,khcd->qhcd", dscore, key_block, preferred_element_type=jnp.float32
            )

        return lax.cond(begin_row <= last_pos, query_compute, lambda sums: sums, partial_value)

    query_sum = lax.fori_loop(0, piece_rows // block_len, query_add_block, running)
    running = (partial_value[1], partial_value[2])
    query_piece = lax.all_gather(queries.astype(jnp.float32), "sp", axis=0, tiled=True).astype(
        jnp.bfloat16
    )
    grad_piece = lax.all_gather(grad_flat.astype(jnp.float32), "sp", axis=0, tiled=True).astype(
        jnp.bfloat16
    )
    log_piece = lax.all_gather(log_sums, "sp", axis=0, tiled=True)
    term_piece = lax.all_gather(term_flat, "sp", axis=0, tiled=True)
    piece_rows = query_piece.shape[0]
    key_block_len = block_span()

    def key_add_block(block_idx, partial_value):
        begin_row = block_idx * key_block_len
        query_block = lax.dynamic_slice_in_dim(query_piece, begin_row, key_block_len, 0).reshape(
            key_block_len, head_count, 2, -1
        )
        grad_block = lax.dynamic_slice_in_dim(grad_piece, begin_row, key_block_len, 0).reshape(
            key_block_len, head_count, -1
        )
        log_block = lax.dynamic_slice_in_dim(log_piece, begin_row, key_block_len, 0).reshape(
            key_block_len, head_count, 2
        )
        term_block = lax.dynamic_slice_in_dim(term_piece, begin_row, key_block_len, 0).reshape(
            key_block_len, head_count, 2
        )
        query_pos = begin_row + jnp.arange(key_block_len, dtype=jnp.int32)

        def key_compute(sums):
            weights, dscore = block_terms(
                query_block,
                key_heads,
                value_heads,
                grad_block,
                log_block,
                term_block,
                lambdas,
                query_pos,
                own_pos,
            )
            key_sum = sums[0] + jnp.einsum(
                "hcqk,qhcd->khcd", dscore, query_block, preferred_element_type=jnp.float32
            )
            value_sum = sums[1] + jnp.einsum(
                "hqk,qhe->khe", weights, grad_block, preferred_element_type=jnp.float32
            )
            return (key_sum, value_sum)

        return lax.cond(
            begin_row + key_block_len - 1 >= offset, key_compute, lambda sums: sums, partial_value
        )

    key_sum, value_sum = lax.fori_loop(0, piece_rows // key_block_len, key_add_block, running)
    value_flat = value_sum.reshape(tok_rows, -1)
    value_narrow = value_flat.astype(jnp.bfloat16)
    weight_grad = sent_and_summed(
        lax.dot_general(
            gathered, value_narrow, (((0,), (0,)), ((), ())), preferred_element_type=jnp.float32
        ),
        "sp",
        0,
    )
    return (query_sum.reshape(tok_rows, -1), key_sum.reshape(tok_rows, -1), value_flat, weight_grad)


def solution(mesh):
    return jax.shard_map(
        per_device,
        mesh=mesh,
        in_specs=(
            P("sp", "tp"),
            P("sp", "tp"),
            P("sp", "tp"),
            P(None, "tp"),
            P("sp", "tp"),
            P("sp", "tp"),
            P("sp", "tp"),
            P("tp"),
            P(),
        ),
        out_specs=(P("sp", "tp"), P("sp", "tp"), P("sp", "tp"), P("sp", "tp")),
        check_vma=False,
    )
```

profile of v0, /device:TPU:230, one launch (start us, length us, event | category | flops | bytes accessed | tf_op | source)
XLA Modules:
  0.0 550.2 jit_solution(8664452942930428712)
XLA Ops:
  13.4 31.5 %all_to_all.10 = bf16[8,512,256]{1,2,0:T(8,128)(2,1)S(1)} all-to-all(bf16[8,512,256]{1,2,0:T(8,128)(2,1)S(1)} %broadcast_in_dim.43), channel_id=1, replica_groups=mesh['sp'=32,'tp'=8] {'tp'}, dimensions={0} | all-to-all | bytes 4194304 | tf_op jit(solution)/shard_map/all_to_all | solution.py:12
  44.8 1.4 convolution_convert_fusion
  46.3 41.4 %all_gather.21 = f32[16384,2]{0,1:T(2,128)S(1)} all-gather(f32[512,2]{0,1:T(2,128)S(1)} %copy-done.8), channel_id=1, replica_groups=mesh['sp'=32,'tp'=8] {'sp'}, dimensions={0}, use_global_device_ids=true | all-gather | bytes 135168 | tf_op jit(solution)/shard_map/all_gather | solution.py:157
  87.7 45.3 %all-gather = f32[16384,1,2]{0,2,1:T(2,128)} all-gather(f32[512,1,2]{0,2,1:T(2,128)S(1)} %pad_maximum_fusion), channel_id=2, replica_groups=mesh['sp'=32,'tp'=8] {'sp'}, dimensions={0}, use_global_device_ids=true | all-gather | bytes 135168 | tf_op jit(solution)/shard_map/all_gather | solution.py:158
  133.0 6.4 %copy.34 = bf16[16384,128]{1,0:T(8,128)(2,1)} copy(bf16[16384,128]{0,1:T(8,128)(2,1)} %all-gather.12.cloned.1.call-done) | data formatting | bytes 8388608
  139.4 41.9 %all-gather.10.cloned.1.call-done = bf16[16384,128]{0,1:T(8,128)(2,1)} async-done(((bf16[512,128]{0,1:T(8,128)(2,1)}), bf16[16384,128]{0,1:T(8,128)(2,1)}) %all-gather.10.cloned.1.call-update) | async-done | bytes 4194320 | tf_op jit(solution)/shard_map/all_gather | solution.py:151
  181.4 8.6 %while.39 = (s32[]{:T(128)}, f32[512,1,2,64]{0,3,2,1:T(8,128)S(1)}, f32[512,1,128]{0,2,1:T(8,128)S(1)}, s32[]{:T(128)}, bf16[16384,128]{0,1:T(8,128)(2,1)}, /*in...) while((s32[]{:T(128)}, f32[512,1,2,64]{0,3,2,1:T(8,128)S(1)}, ...), condition=%wide.region_11.12_spmd.clone.clone, body=%wide.region_8.11_spmd.clone.clone.sunk | while | flops 274072576 | bytes 13155721 | solution.py:202
  183.3 6.7 %conditional.8 = ((f32[512,1,2,64]{0,3,2,1:T(8,128)S(1)}, f32[512,1,128]{0,2,1:T(8,128)S(1)})) conditional(s32[]{:T(128)} %convert_element_type.138, (f32[512,1,2,64]{0,3,2,1:T(8,128)S(1)}, f32[512,1,128]{0,2,1:T(8,128)S(1)}) %tuple.144, (s32[]{:T(128)}, bf16[16384,128]{0,1:T(8,128)(2,1)}, s32[]{:T(128)}, s32[512]{0:T(512)S(1)}, ...), branch_computations={%region_9.9_spmd, %region_10.10_spmd} | conditional | flops 274072576 | bytes 13153374 | solution.py:198
  186.5 1.3 fusion.23
  188.1 1.8 fusion.21
  190.0 1.8 convolution_bitcast_fusion.3
  191.8 2.6 copy.36
  194.4 210.6 %all-to-all-start.1 = ((f32[32,64,128]{2,1,0:T(8,128)}), f32[32,64,128]{2,1,0:T(8,128)S(1)}, u32[]{:S(2)}, u32[]{:S(2)}) async-start(f32[32,64,128]{2,1,0:T(8,128)} %bitcast.64), calls=%async_computation.1 | async-start | bytes 2097152 | tf_op jit(solution)/shard_map/all_to_all | solution.py:34
  406.9 135.3 %while.38 = (s32[]{:T(128)}, f32[512,1,2,64]{0,3,2,1:T(8,128)S(1)}, s32[]{:T(128)}, bf16[16384,128]{0,1:T(8,128)(2,1)}, bf16[512,1,2,64]{0,3,2,1:T(8,128)(2,1)S(...) while((s32[]{:T(128)}, f32[512,1,2,64]{0,3,2,1:T(8,128)S(1)}, ...), condition=%wide.region_7.8_spmd.clone, body=%wide.region_4.7_spmd.clone.sunk | while | flops 206111744 | bytes 10386241 | solution.py:149
  406.9 4.2 conditional.7
  411.2 4.2 conditional.7
  413.8 1.3 fusion.10
  415.4 4.2 conditional.7
  418.0 1.3 fusion.10
  419.6 4.2 conditional.7
  423.8 4.2 conditional.7
  428.1 4.2 conditional.7
  432.3 4.2 conditional.7
  436.5 4.2 conditional.7
  440.8 4.2 conditional.7
  445.0 4.2 conditional.7
  449.2 4.2 conditional.7
  453.4 4.2 conditional.7
  457.7 4.2 conditional.7
  461.9 4.2 conditional.7
  466.1 4.2 conditional.7
  470.3 4.2 conditional.7
  474.6 4.2 conditional.7
  478.8 4.2 conditional.7
  483.0 4.2 conditional.7
  487.3 4.2 conditional.7
  491.5 4.2 conditional.7
  495.7 4.2 conditional.7
  499.9 4.2 conditional.7
  504.2 4.2 conditional.7
  508.4 4.2 conditional.7
  512.6 4.2 conditional.7
  516.8 4.2 conditional.7
  521.1 4.2 conditional.7
  525.3 4.2 conditional.7
  529.5 4.2 conditional.7
  533.8 4.2 conditional.7
  538.0 4.2 conditional.7
  (378 shorter events, 120.8 us)
Async XLA Ops:
  7.2 37.7 %copy-start = (bf16[2048,128]{1,0:T(8,128)(2,1)S(1)}, bf16[2048,128]{1,0:T(8,128)(2,1)}, u32[]{:S(2)}) copy-start(bf16[2048,128]{1,0:T(8,128)(2,1)} %param.20) | copy-start | bytes 1572868
  7.2 3.1 copy-start.9
  7.2 4.1 copy-start.6
  7.2 5.0 copy-start.7
  7.2 125.8 %all-gather.12.cloned.1.call-start = ((), (), s32[]{:S(2)}) async-start(), calls=%async_computation.5 | async-start | bytes 4325376 | tf_op jit(solution)/shard_map/all_gather | solution.py:154
  8.4 4.6 copy-start.5
  11.3 170.1 %all-gather.10.cloned.1.call-start = ((), (), s32[]{:S(2)}) async-start(), calls=%async_computation.4 | async-start | bytes 4325376 | tf_op jit(solution)/shard_map/all_gather | solution.py:151
  12.1 394.8 %all-gather.6.cloned.1.call-start = ((), (), s32[]{:S(2)}) async-start(), calls=%async_computation.2 | async-start | bytes 4325376 | tf_op jit(solution)/shard_map/all_gather | solution.py:112
  13.0 393.9 %all-gather.8.cloned.1.call-start = ((), (), s32[]{:S(2)}) async-start(), calls=%async_computation.3 | async-start | bytes 4325376 | tf_op jit(solution)/shard_map/all_gather | solution.py:115
  44.8 1.5 copy-start.8
  133.0 48.4 %copy-start.1 = (bf16[512,128]{1,0:T(8,128)(2,1)S(1)}, bf16[512,128]{1,0:T(8,128)(2,1)}, u32[]{:S(2)}) copy-start(bf16[512,128]{1,0:T(8,128)(2,1)} %convolution_convert_fusion) | copy-start | bytes 393220
  133.0 48.4 %copy-start.4 = (bf16[512,128]{0,1:T(8,128)(2,1)S(1)}, bf16[512,128]{0,1:T(8,128)(2,1)}, u32[]{:S(2)}) copy-start(bf16[512,128]{0,1:T(8,128)(2,1)} %copy.26) | copy-start | bytes 393220
  191.8 213.3 %copy-start.2 = (bf16[512,128]{0,1:T(8,128)(2,1)S(1)}, bf16[512,128]{0,1:T(8,128)(2,1)}, u32[]{:S(2)}) copy-start(bf16[512,128]{0,1:T(8,128)(2,1)} %get-tuple-element.1056) | copy-start | bytes 393220
  194.4 212.5 %copy-start.3 = (bf16[512,128]{0,1:T(8,128)(2,1)S(1)}, bf16[512,128]{0,1:T(8,128)(2,1)}, u32[]{:S(2)}) copy-start(bf16[512,128]{0,1:T(8,128)(2,1)} %copy.27) | copy-start | bytes 393220
  194.4 348.6 %all-to-all-start.1 = ((f32[32,64,128]{2,1,0:T(8,128)}), f32[32,64,128]{2,1,0:T(8,128)S(1)}, u32[]{:S(2)}, u32[]{:S(2)}) async-start(f32[32,64,128]{2,1,0:T(8,128)} %bitcast.64), calls=%async_computation.1 | async-start | bytes 2097152 | tf_op jit(solution)/shard_map/all_to_all | solution.py:34
Sparse Core Ops, SparseCore 0:
  11.4 84.5 all-gather.11
  98.5 82.7 all-gather.9
  184.4 83.2 all-gather.5
  270.1 78.6 all-gather.7
where the time goes:
time: 554 us; the launch traced here: 550 us
  starting transfers between devices  211 us (38%)
  blocking collectives  118 us (21%)
  matrix products  81.8 us (15%)
  local copies, waits for them, and re-layouts  47.2 us (9%)
  waiting for transfers between devices  42 us (8%)
  loops' own time  26.7 us (5%)
  between operations  14.7 us (3%)
  other arithmetic  8.97 us (2%)
    all_to_all x1, starting transfers between devices, sent_and_summed(): lax.all_to_all(pieces, axis, split_axis=0, concat_axis=0, tiled=True)  211 us
    all_gather x1, blocking collectives, per_device(): term_piece = lax.all_gather(term_flat, 'sp', axis=0, tiled=True)  45.3 us
    all_gather x1, waiting for transfers between devices, per_device(): lax.all_gather(queries.astype(jnp.float32), 'sp', axis=0, tiled=True)  41.9 us
    dot_general x33, matrix products, block_terms(): jnp.einsum('qhe,khe->hqk', grad_block, value_block, preferred_element_typ...  41.8 us
    all_gather x1, blocking collectives, per_device(): log_piece = lax.all_gather(log_sums, 'sp', axis=0, tiled=True)  41.4 us
    all_to_all x1, blocking collectives, sent_to_all(): return lax.all_to_all(copies, axis, split_axis=0, concat_axis=0, tiled=True)  31.5 us
    dynamic_slice x32, local copies, waits for them, and re-layouts, query_add_block(): lax.dynamic_slice_in_dim(key_piece, begin_row, block_len, 0)  29.4 us
    dot_general x33, matrix products, block_terms(): jnp.einsum('qhcd,khcd->hcqk', query_block, key_block, preferred_element_t...  24.8 us
  transfers between devices with their start and end apart: 5, of which 1 were waited for; matrix products, arithmetic and copies ran while one was open for 24% of the time, Pallas kernels for 0%

commit v1 on v0

v1 whole, which is shorter than its diff:
```python
import functools
import math

import jax
import jax.numpy as jnp
import numpy as np
from jax import lax
from jax.experimental import pallas as pl
from jax.experimental.pallas import tpu as pltpu
from jax.sharding import Mesh, PartitionSpec as P

norm_floor = 0.25
log2_e = math.log2(math.e)
f32 = jnp.float32
bf16 = jnp.bfloat16
rows_by_rows = (((1,), (1,)), ((), ()))
rows_by_cols = (((1,), (0,)), ((), ()))
cols_by_cols = (((0,), (0,)), ((), ()))


def head_cotangent(out_pair, cotangent, lam, out_gain):
    first_out = out_pair[:, :128].astype(f32)
    second_out = out_pair[:, 128:].astype(f32)
    merged = first_out - lam * second_out
    inv_norm = lax.rsqrt(jnp.mean(merged * merged, axis=-1, keepdims=True) + norm_floor)
    scaled = cotangent.astype(f32) * out_gain
    inner_dot = jnp.mean(scaled * merged, axis=-1, keepdims=True)
    out_grad = (inv_norm * scaled - merged * (inv_norm * inv_norm * inv_norm) * inner_dot).astype(bf16)
    wide = out_grad.astype(f32)
    return out_grad, jnp.sum(wide * first_out, axis=-1), jnp.sum(wide * second_out, axis=-1)


def attention_kernel(place, query_ref, row_ref, key_ref, dq_ref, dk_ref, dv_ref, *, key_len, tok_len):
    low, col, half = place[0], place[1], place[2]
    dq_ref[...] = jnp.zeros_like(dq_ref)
    dk_ref[...] = jnp.zeros_like(dk_ref)
    dv_ref[...] = jnp.zeros_like(dv_ref)
    first_lanes = lax.broadcasted_iota(jnp.int32, (1, 128), 1) < 64
    first_count = 8 - low

    def split(x):
        zero = jnp.zeros_like(x)
        return jnp.where(first_lanes, x, zero), jnp.where(first_lanes, zero, x)

    def tile(step, masked):
        second = step >= first_count
        group = jnp.where(second, 1, 0)
        block = jnp.where(second, 7 - low + (step - first_count), low + step)
        for tok in range(0, 512, tok_len):
            toks = slice(tok, tok + tok_len)
            query = query_ref[block, toks, 0:128]
            grad = query_ref[block, toks, 128:256]
            query_0, query_1 = split(query)
            log_0, log_1 = row_ref[block, 0:1, toks], row_ref[block, 1:2, toks]
            term_0, term_1 = row_ref[block, 2:3, toks], row_ref[block, 3:4, toks]
            for key in range(0, 1024, key_len):
                keys = slice(key, key + key_len)
                key_0, key_1 = split(key_ref[group, keys, 0:128])
                value = key_ref[group, keys, 128:256]
                score_0 = lax.dot_general(key_0, query, rows_by_rows, preferred_element_type=f32)
                score_1 = lax.dot_general(key_1, query, rows_by_rows, preferred_element_type=f32)
                dot = lax.dot_general(value, grad, rows_by_rows, preferred_element_type=f32)
                map_0 = jnp.exp2(score_0 * (log2_e / 8) - log_0)
                map_1 = jnp.exp2(score_1 * (log2_e / 8) - log_1)
                if masked:
                    row = lax.broadcasted_iota(jnp.int32, (key_len, 1), 0) + key
                    key_pos = (row // 256 - col) * 512 + half * 256 + row % 256
                    tok_pos = lax.broadcasted_iota(jnp.int32, (1, tok_len), 1) + tok
                    visible = key_pos <= tok_pos
                    map_0 = jnp.where(visible, map_0, 0.0)
                    map_1 = jnp.where(visible, map_1, 0.0)
                grad_0 = (map_0 * (dot - term_0)).astype(bf16)
                grad_1 = (map_1 * (term_1 - dot)).astype(bf16)
                mixed = (map_0 - map_1).astype(bf16)
                dk_ref[group, keys, :] += lax.dot_general(
                    grad_0, query_0, rows_by_cols, preferred_element_type=f32
                ) + lax.dot_general(grad_1, query_1, rows_by_cols, preferred_element_type=f32)
                dv_ref[group, keys, :] += lax.dot_general(
                    mixed, grad, rows_by_cols, preferred_element_type=f32
                )
                dq_ref[block, toks, :] += lax.dot_general(
                    grad_0, key_0, cols_by_cols, preferred_element_type=f32
                ) + lax.dot_general(grad_1, key_1, cols_by_cols, preferred_element_type=f32)

    def one_step(step, carry):
        diagonal = (step == 0) | (step == first_count)
        pl.when(diagonal)(lambda: tile(step, True))
        pl.when(jnp.logical_not(diagonal))(lambda: tile(step, False))
        return carry

    lax.fori_loop(0, 9, one_step, 0)


def attention(place, queries, rows, keys):
    vmem = pl.BlockSpec(memory_space=pltpu.VMEM)
    return pl.pallas_call(
        functools.partial(attention_kernel, key_len=512, tok_len=256),
        out_shape=(
            jax.ShapeDtypeStruct((8, 512, 128), f32),
            jax.ShapeDtypeStruct((2, 1024, 128), f32),
            jax.ShapeDtypeStruct((2, 1024, 128), f32),
        ),
        in_specs=[pl.BlockSpec(memory_space=pltpu.SMEM), vmem, vmem, vmem],
        out_specs=[vmem, vmem, vmem],
        compiler_params=pltpu.CompilerParams(vmem_limit_bytes=60 * 1024 * 1024),
        cost_estimate=pl.CostEstimate(flops=9 * 1024 * 512 * 2048, bytes_accessed=8 << 20, transcendentals=0),
        name="attention",
    )(place, queries, rows, keys)


def per_device(queries, key_vectors, latents, w_value, log_sums, out_pair, cotangent, lambdas, out_gain):
    z, x = lax.axis_index("z"), lax.axis_index("x")
    lam = lambdas[0]
    low = jnp.minimum(z, 7 - z)
    half = jnp.where(z < 4, 0, 1)
    mirror = [(i, 7 - i) for i in range(8)]

    out_grad, first_term, second_term = head_cotangent(out_pair, cotangent, lam, out_gain)
    rows = jnp.stack(
        [log_sums[:, 0] * log2_e, log_sums[:, 1] * log2_e - jnp.log2(lam), first_term, second_term]
    )
    query_all = lax.all_gather(jnp.concatenate([queries, out_grad], axis=1), "z")
    row_all = lax.all_gather(rows, "z")

    latents_all = lax.all_gather(latents, ("y", "core"), axis=1, tiled=True)
    values = jnp.dot(latents_all, w_value, preferred_element_type=f32).astype(bf16)
    pair = jnp.concatenate([key_vectors, values], axis=1).reshape(2, 256, 256)
    kept = lax.dynamic_index_in_dim(pair, half, 0, keepdims=False)
    given = lax.dynamic_index_in_dim(pair, 1 - half, 0, keepdims=False)
    came = lax.ppermute(given, "z", mirror)
    upper = z >= 4
    key_two = jnp.stack([jnp.where(upper, came, kept), jnp.where(upper, kept, came)])
    key_all = lax.all_gather(key_two, "x", axis=1).reshape(2, 1024, 256)

    place = jnp.stack([low, x, half]).astype(jnp.int32)
    dq, dk, dv = attention(place, query_all, row_all, key_all)

    query_grad = lax.psum_scatter(dq, "z", scatter_dimension=0) * 0.125
    both = jnp.concatenate([dk * 0.125, dv], axis=-1).reshape(2, 4, 256, 256)
    own = lax.psum_scatter(both, "x", scatter_dimension=1)
    kept = jnp.where(upper, own[1], own[0])
    given = jnp.where(upper, own[0], own[1])
    came = lax.ppermute(given, "z", mirror)
    whole = jnp.concatenate([jnp.where(upper, came, kept), jnp.where(upper, kept, came)])
    key_grad, value_grad = whole[:, :128], whole[:, 128:]
    partial = lax.dot_general(
        latents_all, value_grad.astype(bf16), cols_by_cols, preferred_element_type=f32
    )
    weight_grad = lax.psum_scatter(partial, ("z", "x"), scatter_dimension=0, tiled=True)
    return query_grad, key_grad, value_grad, weight_grad


def solution(mesh):
    grid = Mesh(mesh.devices.reshape(8, 4, 4, 2), ("z", "x", "y", "core"))
    sp, tp = ("z", "x"), ("y", "core")
    return jax.shard_map(
        per_device,
        mesh=grid,
        in_specs=(
            P(sp, tp),
            P(sp, tp),
            P(sp, tp),
            P(None, tp),
            P(sp, tp),
            P(sp, tp),
            P(sp, tp),
            P(tp),
            P(),
        ),
        out_specs=(P(sp, tp), P(sp, tp), P(sp, tp), P(sp, tp)),
        check_vma=False,
    )
```

time: 554 us -> 482 us (0.87)
  the two profiles are of different devices: /device:TPU:230 before, /device:TPU:8 now
where the time goes in v1:
time: 482 us
  waiting for transfers between devices  382 us (79%)
  Pallas kernels  28.2 us (6%)
  blocking collectives  27.4 us (6%)
  between operations  15 us (3%)
  other arithmetic  14.5 us (3%)
  starting transfers between devices  7.04 us (1%)
    unnamed x8, waiting for transfers between devices  283 us
    all_gather x1, waiting for transfers between devices, per_device(): latents_all = lax.all_gather(latents, ('y', 'core'), axis=1, tiled=True)  28.3 us
    pallas_call x1, Pallas kernels, attention(): pl.pallas_call(functools.partial(attention_kernel, key_len=512, tok_len=2...  28.2 us
    all_gather x1, waiting for transfers between devices, per_device(): key_all = lax.all_gather(key_two, 'x', axis=1).reshape(2, 1024, 256)  27.9 us
    all_gather x1, blocking collectives, per_device(): row_all = lax.all_gather(rows, 'z')  27.4 us
    ppermute x2, waiting for transfers between devices, per_device(): came = lax.ppermute(given, 'z', mirror)  21.2 us
    reduce_scatter x1, waiting for transfers between devices, per_device(): query_grad = lax.psum_scatter(dq, 'z', scatter_dimension=0) * 0.125  18.6 us
  transfers between devices with their start and end apart: 8, of which 8 were waited for; matrix products, arithmetic and copies ran while one was open for 4% of the time, Pallas kernels for 0%

profile of v1, /device:TPU:8, one launch (start us, length us, event | category | flops | bytes accessed | tf_op | source)
XLA Modules:
  0.0 482.0 jit_solution(4503313385731957119)
XLA Ops:
  7.2 0.0 copy-start
  7.2 0.0 all-gather.8.cloned.1.call-start
  7.2 0.7 all-gather.8.cloned.1.call-update
  7.9 0.0 all-gather.10.cloned.1.call-start
  8.6 1.3 multiply_reduce_fusion.1
  9.9 1.5 fusion
  11.4 1.6 pad_maximum_fusion.2
  13.1 0.0 all-gather.10.cloned.1.call-update
  13.1 0.0 all-gather.12.cloned.1.call-start
  13.1 0.0 copy-done.4
  13.1 0.1 copy.17
  13.3 0.0 copy-start.5
  13.3 28.3 %all-gather.8.cloned.1.call-done = bf16[512,2048]{1,0:T(8,128)(2,1)} async-done(((bf16[512,256]{1,0:T(8,128)(2,1)}), bf16[512,2048]{1,0:T(8,128)(2,1)}) %all-gather.8.cloned.1.call-update) | async-done | bytes 2097168 | tf_op jit(solution)/shard_map/all_gather | solution.py:125
  41.6 0.0 copy-done
  41.6 2.4 convolution_convert_fusion
  44.0 0.1 copy.25
  44.2 3.4 collective-permute-start
  47.6 6.7 %collective-permute-done = bf16[256,256]{1,0:T(8,128)(2,1)S(1)} collective-permute-done((bf16[256,256]{1,0:T(8,128)(2,1)S(1)}, bf16[256,256]{1,0:T(8,128)(2,1)S(1)}, u32[]{:S(2)}, u32[]{:S(2)}) %collective-permute-start) | collective-permute-done | bytes 131104 | tf_op jit(solution)/shard_map/ppermute | solution.py:130
  54.4 0.7 pad_maximum_fusion.4
  55.1 0.0 all-gather.12.cloned.1.call-update
  55.1 0.0 all-reduce.3.cloned.1.call-start
  55.3 27.4 %all-gather.3.row_ref = f32[8,4,512]{2,1,0:T(4,128)} all-gather(f32[1,4,512]{2,1,0:T(4,128)S(1)} %maximum_bitcast_fusion), channel_id=3, replica_groups=mesh['z'=8,'x'=4,'y'=4,'core'=2] {'z'}, dimensions={0}, use_global_device_ids=true | all-gather | bytes 73728 | tf_op jit(solution)/shard_map/all_gather | solution.py:123
  82.7 0.6 pad_add_fusion.place
  83.2 3.0 all-gather.10.cloned.1.call-done
  86.2 27.9 %all-gather.12.cloned.1.call-done.key_ref = bf16[2,1024,256]{2,1,0:T(8,128)(2,1)} async-done(((bf16[2,256,256]{2,1,0:T(8,128)(2,1)}), bf16[2,1024,256]{2,1,0:T(8,128)(2,1)}) %all-gather.12.cloned.1.call-update) | async-done | bytes 1048592 | tf_op jit(solution)/shard_map/all_gather | solution.py:133
  114.2 28.2 %attention.1 = (f32[8,512,128]{2,1,0:T(8,128)}, f32[2,1024,128]{2,1,0:T(8,128)}, f32[2,1024,128]{2,1,0:T(8,128)}) custom-call(s32[3]{0:T(128)} %pad_add_fusion.place, bf16[8,512,256]{2,1,0:T(8,128)(2,1)} %bitcast.56, f32[8,4,512]{2,1,0:T(4,128)} %all-gather.3.row_ref, bf16[2,1024,256]{2,1,0:T(8,128)(2,1)} %all-gather.12.cloned.1.call-done.key_ref), custom_call_target="tpu_custom_call" | custom-call | flops 9663676416 | bytes 8388608 | tf_op jit(solution)/shard_map/attention/pallas_call | solution.py:96
  142.4 1.4 broadcast_multiply_fusion
  143.7 0.2 copy-done.2
  143.9 1.5 pad_maximum_fusion
  145.4 0.0 all-reduce.3.cloned.1.call-update
  145.4 0.0 reduce-scatter.8.cloned.1.call-start
  145.4 0.5 reduce-scatter.8.cloned.1.call-update
  146.0 0.0 reduce-scatter.10.cloned.1.call-start
  146.1 0.0 copy-done.6
  146.1 0.6 dynamic-slice
  146.6 63.0 %all-reduce.3.cloned.1.call-done = f32[2,4,256,256]{3,2,1,0:T(8,128)} async-done(((f32[2,4,256,256]{3,2,1,0:T(8,128)}), f32[2,4,256,256]{3,2,1,0:T(8,128)}) %all-reduce.3.cloned.1.call-update) | async-done | bytes 2097168
  209.7 1.7 select_bitcast_fusion
  211.4 3.4 collective-permute-start.1
  214.8 14.5 %collective-permute-done.1 = f32[256,256]{1,0:T(8,128)S(1)} collective-permute-done((f32[256,256]{1,0:T(8,128)S(1)}, f32[256,256]{1,0:T(8,128)S(1)}, u32[]{:S(2)}, u32[]{:S(2)}) %collective-permute-start.1) | collective-permute-done | bytes 262176 | tf_op jit(solution)/shard_map/ppermute | solution.py:143
  229.3 1.7 bitcast_select_fusion
  231.0 0.7 pad_maximum_fusion.1
  231.7 0.0 copy-done.1
  231.7 1.5 convolution_bitcast_fusion
  233.2 2.6 copy.23
  235.8 0.0 reduce-scatter.10.cloned.1.call-update
  235.8 18.6 %reduce-scatter.8.cloned.1.call-done = f32[1,512,128]{2,1,0:T(8,128)} async-done(((f32[8,512,128]{2,1,0:T(8,128)}), f32[1,512,128]{2,1,0:T(8,128)}) %reduce-scatter.8.cloned.1.call-update) | async-done | bytes 262160 | tf_op jit(solution)/shard_map/reduce_scatter | solution.py:138
  254.4 1.7 multiply_bitcast_fusion
  256.1 219.1 %reduce-scatter.10.cloned.1.call-done = f32[64,128]{1,0:T(8,128)} async-done(((f32[2048,128]{1,0:T(8,128)}), f32[64,128]{1,0:T(8,128)}) %reduce-scatter.10.cloned.1.call-update) | async-done | bytes 32784
  (13 shorter events, 0.1 us)
Async XLA Ops:
  7.2 34.4 %copy-start = (bf16[2048,128]{1,0:T(8,128)(2,1)S(1)}, bf16[2048,128]{1,0:T(8,128)(2,1)}, u32[]{:S(2)}) copy-start(bf16[2048,128]{1,0:T(8,128)(2,1)} %param.12) | copy-start | bytes 1572868
  7.2 6.0 %copy-start.4 = (bf16[512,128]{1,0:T(8,128)(2,1)S(1)}, bf16[512,128]{1,0:T(8,128)(2,1)}, u32[]{:S(2)}) copy-start(bf16[512,128]{1,0:T(8,128)(2,1)} %param.10) | copy-start | bytes 393220
  7.2 34.4 %all-gather.8.cloned.1.call-start = ((), (), s32[]{:S(2)}) async-start(), calls=%async_computation.2 | async-start | bytes 2359296 | tf_op jit(solution)/shard_map/all_gather | solution.py:125
  7.9 78.3 %all-gather.10.cloned.1.call-start = ((), (), s32[]{:S(2)}) async-start(), calls=%async_computation.4 | async-start | bytes 2359296 | tf_op jit(solution)/shard_map/all_gather | solution.py:122
  13.1 101.1 %all-gather.12.cloned.1.call-start = ((), (), s32[]{:S(2)}) async-start(), calls=%async_computation.5 | async-start | bytes 1310720 | tf_op jit(solution)/shard_map/all_gather | solution.py:133
  13.3 41.9 %copy-start.5 = (f32[512,2]{0,1:T(2,128)S(1)}, f32[512,2]{0,1:T(2,128)}, u32[]{:S(2)}) copy-start(f32[512,2]{0,1:T(2,128)} %param.13) | copy-start | bytes 12292
  44.2 10.1 %collective-permute-start = (bf16[256,256]{1,0:T(8,128)(2,1)S(1)}, bf16[256,256]{1,0:T(8,128)(2,1)S(1)}, u32[]{:S(2)}, u32[]{:S(2)}) collective-permute-start(bf16[256,256]{1,0:T(8,128)(2,1)S(1)} %dynamic-slice_bitcast_fusion), channel_id=1, source_target_pairs={{0,224},{32,192},{64,160},{96,128},{128,96},{160,64},{192,32},{224... | collective-permute-start | bytes 393224 | tf_op jit(solution)/shard_map/ppermute | solution.py:130
  55.1 154.6 %all-reduce.3.cloned.1.call-start = ((), (), s32[]{:S(2)}) async-start(), calls=%async_computation.7 | async-start | bytes 4194304
  142.4 1.5 copy-start.2
  145.4 0.7 copy-start.6
  145.4 109.0 %reduce-scatter.8.cloned.1.call-start = ((), (), s32[]{:S(2)}) async-start(), calls=%async_computation.3 | async-start | bytes 2359296 | tf_op jit(solution)/shard_map/reduce_scatter | solution.py:138
  146.0 85.8 %copy-start.1 = (bf16[512,2048]{1,0:T(8,128)(2,1)S(1)}, bf16[512,2048]{1,0:T(8,128)(2,1)}, u32[]{:S(2)}) copy-start(bf16[512,2048]{1,0:T(8,128)(2,1)} %all-gather.8.cloned.1.call-done) | copy-start | bytes 6291460
  146.0 329.2 %reduce-scatter.10.cloned.1.call-start = ((), (), s32[]{:S(2)}) async-start(), calls=%async_computation.6 | async-start | bytes 1081344
  211.4 17.9 %collective-permute-start.1 = (f32[256,256]{1,0:T(8,128)S(1)}, f32[256,256]{1,0:T(8,128)S(1)}, u32[]{:S(2)}, u32[]{:S(2)}) collective-permute-start(f32[256,256]{1,0:T(8,128)S(1)} %select_bitcast_fusion), channel_id=1, source_target_pairs={{0,224},{32,192},{64,160},{96,128},{128,96},{160,64},{192,32},{224... | collective-permute-start | bytes 786440 | tf_op jit(solution)/shard_map/ppermute | solution.py:143
  231.7 4.0 copy-start.3
Sparse Core Ops, SparseCore 0:
  9.8 31.7 all-gather.7
  44.0 42.2 all-gather.9
  88.6 25.4 all-gather.11
  145.5 64.1 all-reduce.2
  212.1 42.2 reduce-scatter.7
  258.7 216.4 reduce-scatter.9

commit v2 on v1

--- a/solution.py
+++ b/solution.py
@@ -30,7 +30,197 @@
     return out_grad, jnp.sum(wide * first_out, axis=-1), jnp.sum(wide * second_out, axis=-1)
 
 
-def attention_kernel(place, query_ref, row_ref, key_ref, dq_ref, dk_ref, dv_ref, *, key_len, tok_len):
+mesh_ids = pl.DeviceIdType.MESH
+
+
+class Sender:
+    def __init__(self, send_sems, recv_sems):
+        self.send_sems, self.recv_sems, self.copies = send_sems, recv_sems, {}
+
+    def start(self, name, source, target, device):
+        place = len(self.copies)
+        copy = pltpu.make_async_remote_copy(
+            src_ref=source,
+            dst_ref=target,
+            send_sem=self.send_sems.at[place],
+            recv_sem=self.recv_sems.at[place],
+            device_id=device,
+            device_id_type=mesh_ids,
+        )
+        self.copies[name] = copy
+        copy.start()
+
+    def arrived(self, name):
+        self.copies[name].wait_recv()
+
+    def finish(self):
+        for copy in self.copies.values():
+            copy.wait_send()
+
+
+def greet(devices):
+    barrier = pltpu.get_barrier_semaphore()
+    for device in devices:
+        pl.semaphore_signal(barrier, inc=1, device_id=device, device_id_type=mesh_ids)
+    pl.semaphore_wait(barrier, len(devices))
+
+
+def gather_kernel(
+    query_ref, row_ref, latent_ref, weight_ref, key_ref,
+    query_all, row_all, latent_all, key_all, value_all,
+    value_own, send_sems, recv_sems,
+):
+    z, x, y, core = (lax.axis_index(name) for name in ("z", "x", "y", "core"))
+    up, down = {"z": lax.rem(z + 1, 8)}, {"z": lax.rem(z + 7, 8)}
+    mirror = {"z": 7 - z}
+    right, left = {"x": lax.rem(x + 1, 4)}, {"x": lax.rem(x + 3, 4)}
+    ahead, behind = {"y": lax.rem(y + 1, 4)}, {"y": lax.rem(y + 3, 4)}
+    partner = {"core": 1 - core}
+    greet([up, down, mirror, right, left, ahead, behind, partner])
+    sender = Sender(send_sems, recv_sems)
+    start, arrived = sender.start, sender.arrived
+    group = jnp.where(z < 4, 0, 1)
+    half = group
+    halves = (pl.ds(0, 256), pl.ds(256, 256))
+
+    def latent_slot(step, part):
+        slot = lax.rem(y + step + 4, 4) * 2 + core
+        return latent_all.at[slot, halves[part]]
+
+    def latent_to_partner(step, part):
+        start(("pair", step, part), latent_slot(step, part), latent_slot(step, part), partner)
+
+    def query_slot(step, part):
+        return query_all.at[lax.rem(z + step + 8, 8), halves[part]]
+
+    def send_query(way, hops, part):
+        device, sign = (up, -1) if way == "up" else (down, 1)
+        source = query_ref.at[halves[part]] if hops == 0 else query_slot(sign * hops, part)
+        start((way, hops, part), source, query_slot(sign * hops, part), device)
+
+    def send_rows(way, hops):
+        device, sign = (up, -1) if way == "up" else (down, 1)
+        slot = row_all.at[lax.rem(z + sign * hops + 8, 8)]
+        start((way, hops, "rows"), row_ref if hops == 0 else slot, slot, device)
+
+    def pass_query(hops, step):
+        for way, part in (("up", step), ("down", 1 - step)):
+            arrived((way, hops, part))
+            if hops < 2 or (hops == 2 and step == 0):
+                send_query(way, hops + 1, part)
+            if step == 0 and hops < (4 if way == "up" else 3):
+                arrived((way, hops, "rows"))
+                if hops < (3 if way == "up" else 2):
+                    send_rows(way, hops + 1)
+
+    def open_share(name, whole, target):
+        start((name, "mirror"), whole.at[1 - half], target.at[group, x], mirror)
+        start((name, "own", "right"), whole.at[half], target.at[group, x], right)
+        start((name, "own", "left"), whole.at[half], target.at[group, x], left)
+
+    def share_mirrored(name, target):
+        arrived((name, "mirror"))
+        slot = target.at[1 - group, x]
+        start((name, "other", "left"), slot, slot, left)
+        start((name, "other", "right"), slot, slot, right)
+
+    def share_far(name, target):
+        arrived((name, "own", "right"))
+        slot = target.at[group, lax.rem(x + 3, 4)]
+        start((name, "own", "far"), slot, slot, right)
+        arrived((name, "other", "left"))
+        slot = target.at[1 - group, lax.rem(x + 1, 4)]
+        start((name, "other", "far"), slot, slot, left)
+
+    def close_share(name):
+        arrived((name, "own", "left"))
+        arrived((name, "other", "right"))
+        arrived((name, "own", "far"))
+        arrived((name, "other", "far"))
+
+    own_slot = y * 2 + core
+    for way, part, device in (("ahead", 0, ahead), ("behind", 1, behind), ("ahead", 1, ahead), ("behind", 0, behind)):
+        start((way, part), latent_ref.at[halves[part]], latent_all.at[own_slot, halves[part]], device)
+    start("pair", latent_ref, latent_all.at[own_slot], partner)
+    send_query("up", 0, 0)
+    send_query("down", 0, 1)
+    send_rows("up", 0)
+    send_rows("down", 0)
+    open_share("key", key_ref, key_all)
+    send_query("up", 0, 1)
+    send_query("down", 0, 0)
+    latent_all[own_slot] = latent_ref[...]
+    query_all[z] = query_ref[...]
+    row_all[z] = row_ref[...]
+    key_all[group, x] = key_ref[half]
+
+    arrived(("ahead", 0))
+    start(("ahead", "far"), latent_slot(-1, 0), latent_slot(-1, 0), ahead)
+    latent_to_partner(-1, 0)
+    arrived(("behind", 1))
+    start(("behind", "far"), latent_slot(1, 1), latent_slot(1, 1), behind)
+    latent_to_partner(1, 1)
+    pass_query(0, 0)
+    share_mirrored("key", key_all)
+    arrived(("ahead", 1))
+    latent_to_partner(-1, 1)
+    arrived(("behind", 0))
+    latent_to_partner(1, 0)
+    pass_query(0, 1)
+    share_far("key", key_all)
+    arrived(("ahead", "far"))
+    latent_to_partner(2, 0)
+    arrived(("behind", "far"))
+    latent_to_partner(2, 1)
+    pass_query(1, 0)
+    arrived("pair")
+    for step in (-1, 1, 2):
+        for part in (0, 1):
+            arrived(("pair", step, part))
+    total = jnp.zeros((512, 128), f32)
+    for slot in range(8):
+        total += jnp.dot(latent_all[slot], weight_ref[slot], preferred_element_type=f32)
+    own = total.astype(bf16).reshape(2, 256, 128)
+    value_own[...] = own
+    open_share("value", value_own, value_all)
+    value_all[group, x] = value_own[half]
+    pass_query(1, 1)
+    share_mirrored("value", value_all)
+    pass_query(2, 0)
+    share_far("value", value_all)
+    pass_query(2, 1)
+    close_share("key")
+    close_share("value")
+    pass_query(3, 0)
+    sender.finish()
+
+
+def gather(queries, rows, latents, w_value, keys):
+    vmem = pl.BlockSpec(memory_space=pltpu.VMEM)
+    return pl.pallas_call(
+        gather_kernel,
+        out_shape=(
+            jax.ShapeDtypeStruct((8, 512, 256), bf16),
+            jax.ShapeDtypeStruct((8, 8, 512), f32),
+            jax.ShapeDtypeStruct((8, 512, 256), bf16),
+            jax.ShapeDtypeStruct((2, 4, 256, 128), bf16),
+            jax.ShapeDtypeStruct((2, 4, 256, 128), bf16),
+        ),
+        in_specs=[vmem] * 5,
+        out_specs=[vmem] * 5,
+        scratch_shapes=[
+            pltpu.VMEM((2, 256, 128), bf16),
+            pltpu.SemaphoreType.DMA((48,)),
+            pltpu.SemaphoreType.DMA((48,)),
+        ],
+        compiler_params=pltpu.CompilerParams(
+            collective_id=0, has_side_effects=True, vmem_limit_bytes=40 * 1024 * 1024
+        ),
+        name="gather",
+    )(queries, rows, latents, w_value, keys)
+
+
+def attention_kernel(place, query_ref, row_ref, key_ref, value_ref, dq_ref, dk_ref, dv_ref, *, key_len, tok_len):
     low, col, half = place[0], place[1], place[2]
     dq_ref[...] = jnp.zeros_like(dq_ref)
     dk_ref[...] = jnp.zeros_like(dk_ref)
@@ -55,8 +245,8 @@
             term_0, term_1 = row_ref[block, 2:3, toks], row_ref[block, 3:4, toks]
             for key in range(0, 1024, key_len):
                 keys = slice(key, key + key_len)
-                key_0, key_1 = split(key_ref[group, keys, 0:128])
-                value = key_ref[group, keys, 128:256]
+                key_0, key_1 = split(key_ref[group, keys, :])
+                value = value_ref[group, keys, :]
                 score_0 = lax.dot_general(key_0, query, rows_by_rows, preferred_element_type=f32)
                 score_1 = lax.dot_general(key_1, query, rows_by_rows, preferred_element_type=f32)
                 dot = lax.dot_general(value, grad, rows_by_rows, preferred_element_type=f32)
@@ -91,7 +281,7 @@
     lax.fori_loop(0, 9, one_step, 0)
 
 
-def attention(place, queries, rows, keys):
+def attention(place, queries, rows, keys, values):
     vmem = pl.BlockSpec(memory_space=pltpu.VMEM)
     return pl.pallas_call(
         functools.partial(attention_kernel, key_len=512, tok_len=256),
@@ -100,12 +290,12 @@
             jax.ShapeDtypeStruct((2, 1024, 128), f32),
             jax.ShapeDtypeStruct((2, 1024, 128), f32),
         ),
-        in_specs=[pl.BlockSpec(memory_space=pltpu.SMEM), vmem, vmem, vmem],
+        in_specs=[pl.BlockSpec(memory_space=pltpu.SMEM), vmem, vmem, vmem, vmem],
         out_specs=[vmem, vmem, vmem],
         compiler_params=pltpu.CompilerParams(vmem_limit_bytes=60 * 1024 * 1024),
         cost_estimate=pl.CostEstimate(flops=9 * 1024 * 512 * 2048, bytes_accessed=8 << 20, transcendentals=0),
         name="attention",
-    )(place, queries, rows, keys)
+    )(place, queries, rows, keys, values)
 
 
 def per_device(queries, key_vectors, latents, w_value, log_sums, out_pair, cotangent, lambdas, out_gain):
@@ -119,21 +309,18 @@
     rows = jnp.stack(
         [log_sums[:, 0] * log2_e, log_sums[:, 1] * log2_e - jnp.log2(lam), first_term, second_term]
     )
-    query_all = lax.all_gather(jnp.concatenate([queries, out_grad], axis=1), "z")
-    row_all = lax.all_gather(rows, "z")
-
-    latents_all = lax.all_gather(latents, ("y", "core"), axis=1, tiled=True)
-    values = jnp.dot(latents_all, w_value, preferred_element_type=f32).astype(bf16)
-    pair = jnp.concatenate([key_vectors, values], axis=1).reshape(2, 256, 256)
-    kept = lax.dynamic_index_in_dim(pair, half, 0, keepdims=False)
-    given = lax.dynamic_index_in_dim(pair, 1 - half, 0, keepdims=False)
-    came = lax.ppermute(given, "z", mirror)
+    query_all, row_all, latent_all, key_all, value_all = gather(
+        jnp.concatenate([queries, out_grad], axis=1),
+        jnp.concatenate([rows, jnp.zeros_like(rows)]),
+        latents,
+        w_value.reshape(8, 256, 128),
+        key_vectors.reshape(2, 256, 128),
+    )
     upper = z >= 4
-    key_two = jnp.stack([jnp.where(upper, came, kept), jnp.where(upper, kept, came)])
-    key_all = lax.all_gather(key_two, "x", axis=1).reshape(2, 1024, 256)
-
     place = jnp.stack([low, x, half]).astype(jnp.int32)
-    dq, dk, dv = attention(place, query_all, row_all, key_all)
+    dq, dk, dv = attention(
+        place, query_all, row_all, key_all.reshape(2, 1024, 128), value_all.reshape(2, 1024, 128)
+    )
 
     query_grad = lax.psum_scatter(dq, "z", scatter_dimension=0) * 0.125
     both = jnp.concatenate([dk * 0.125, dv], axis=-1).reshape(2, 4, 256, 256)
@@ -144,8 +331,8 @@
     whole = jnp.concatenate([jnp.where(upper, came, kept), jnp.where(upper, kept, came)])
     key_grad, value_grad = whole[:, :128], whole[:, 128:]
     partial = lax.dot_general(
-        latents_all, value_grad.astype(bf16), cols_by_cols, preferred_element_type=f32
-    )
+        latent_all, value_grad.astype(bf16), (((1,), (0,)), ((), ())), preferred_element_type=f32
+    ).reshape(2048, 128)
     weight_grad = lax.psum_scatter(partial, ("z", "x"), scatter_dimension=0, tiled=True)
     return query_grad, key_grad, value_grad, weight_grad
 

time: 482 us -> 397 us (0.82)
  waiting for transfers between devices: 382 us -> 287 us
  Pallas kernels: 28.2 us -> 66.8 us
  blocking collectives: 27.4 us -> 0 us
    unnamed x8 -> x4, waiting for transfers between devices: 283 us -> 60.3 us
    reduce_scatter x0 -> x1, waiting for transfers between devices: none -> 215 us  [per_device(): lax.psum_scatter(partial, ('z', 'x'), scatter_dimension=0, tiled=True)]
    all_gather x3 -> x0, waiting for transfers between devices: 59.2 us -> none  [the longest x1 28.3 us: per_device(): latents_all = lax.all_gather(latents, ('y', 'core'), axis=1, tiled=True)]
    pallas_call x0 -> x1, Pallas kernels: none -> 38.8 us  [gather(): pl.pallas_call(gather_kernel, out_shape=(jax.ShapeDtypeStruct((8, 512, 25...]
    all_gather x1 -> x0, blocking collectives: 27.4 us -> none  [per_device(): row_all = lax.all_gather(rows, 'z')]
    reduce_scatter x1, waiting for transfers between devices: 18.6 us -> 0.03 us  [per_device(): query_grad = lax.psum_scatter(dq, 'z', scatter_dimension=0) * 0.125]
    ppermute x2 -> x1, waiting for transfers between devices: 21.2 us -> 11.8 us  [per_device(): came = lax.ppermute(given, 'z', mirror)]
  transfers between devices with their start and end apart: 8 -> 4, of which waited for: 8 -> 3; matrix products, arithmetic and copies ran while one was open for 4% -> 2% of each run, Pallas kernels for 0% -> 0%
where the time goes in v2:
time: 397 us
  waiting for transfers between devices  287 us (72%)
  Pallas kernels  66.8 us (17%)
  between operations  16.3 us (4%)
  other arithmetic  13.8 us (3%)
  local copies, waits for them, and re-layouts  7.24 us (2%)
    reduce_scatter x1, waiting for transfers between devices, per_device(): lax.psum_scatter(partial, ('z', 'x'), scatter_dimension=0, tiled=True)  215 us
    unnamed x4, waiting for transfers between devices  60.3 us
    pallas_call x1, Pallas kernels, gather(): pl.pallas_call(gather_kernel, out_shape=(jax.ShapeDtypeStruct((8, 512, 25...  38.8 us
    pallas_call x1, Pallas kernels, attention(): pl.pallas_call(functools.partial(attention_kernel, key_len=512, tok_len=2...  28 us
    ppermute x1, waiting for transfers between devices, per_device(): came = lax.ppermute(given, 'z', mirror)  11.8 us
  transfers between devices with their start and end apart: 4, of which 3 were waited for; matrix products, arithmetic and copies ran while one was open for 2% of the time, Pallas kernels for 0%

profile of v2, /device:TPU:8, one launch (start us, length us, event | category | flops | bytes accessed | tf_op | source)
XLA Modules:
  0.0 396.5 jit_solution(16964831490012142073)
XLA Ops:
  8.0 0.0 all-reduce.3.cloned.1.call-start
  8.7 1.3 multiply_reduce_fusion.1
  10.0 0.8 subtract_bitcast_fusion
  10.8 1.5 fusion.1
  12.3 0.9 pad_maximum_fusion.2.query_ref
  13.2 0.6 pad_add_fusion.place
  13.9 0.0 copy-start
  13.9 1.0 copy-done
  14.9 0.0 copy-start.1
  14.9 0.9 copy-done.1
  15.9 0.0 copy-start.2
  15.9 0.9 copy-done.2
  16.8 38.8 %gather.1 = (bf16[8,512,256]{2,1,0:T(8,128)(2,1)S(1)}, f32[8,8,512]{2,1,0:T(8,128)S(1)}, bf16[8,512,256]{2,1,0:T(8,128)(2,1)S(1)}, bf16[2,4,256,128]{3,2,1,0:T(8,128)(2,1)S(1)}, bf16[2,4,256,128]{3,2,1,0:T(8,128)(2,1)S(1)}) custom-call(bf16[512,256]{1,0:T(8,128)(2,1)S(1)} %pad_maximum_fusion.2.query_ref, f32[8,512]{1,0:T(8,128)S(1)} %concatenate.13.row_ref, ...), custom_call_target="tpu_custom_call" | custom-call | tf_op jit(solution)/shard_map/gather/pallas_call | solution.py:200
  55.5 0.0 copy-start.3
  55.5 1.3 copy-done.3
  56.8 0.0 copy-start.4
  56.9 0.8 copy-done.4
  57.7 0.0 copy-start.5
  57.7 0.8 copy-done.5
  58.5 0.0 copy-start.6
  58.5 0.7 copy-done.6
  59.1 28.0 %attention.1 = (f32[8,512,128]{2,1,0:T(8,128)}, f32[2,1024,128]{2,1,0:T(8,128)}, f32[2,1024,128]{2,1,0:T(8,128)}) custom-call(s32[3]{0:T(128)} %pad_add_fusion.place, bf16[8,512,256]{2,1,0:T(8,128)(2,1)} %copy-done.3, f32[8,8,512]{2,1,0:T(8,128)} %copy-done.6, bf16[2,1024,128]{2,1,0:T(8,128)(2,1)} %bitcast.39, bf16[2,1024,128]{2,1,0:T(8,128)(2,1)} %bitcast.40), custom_call_target="tpu_custom_call" | custom-call | flops 9663676416 | bytes 8388608 | tf_op jit(solution)/shard_map/attention/pallas_call | solution.py:286
  87.1 0.0 copy-start.7
  87.1 1.4 broadcast_multiply_fusion
  88.5 0.2 copy-done.7
  88.7 1.5 pad_maximum_fusion
  90.1 0.0 copy-start.9
  90.1 0.0 all-reduce.3.cloned.1.call-update
  90.1 0.0 reduce-scatter.6.cloned.1.call-start
  90.2 0.5 reduce-scatter.6.cloned.1.call-update
  90.7 0.0 reduce-scatter.8.cloned.1.call-start
  90.8 0.0 copy-done.9
  90.8 0.6 dynamic-slice
  91.4 59.7 %all-reduce.3.cloned.1.call-done = f32[2,4,256,256]{3,2,1,0:T(8,128)} async-done(((f32[2,4,256,256]{3,2,1,0:T(8,128)}), f32[2,4,256,256]{3,2,1,0:T(8,128)}) %all-reduce.3.cloned.1.call-update) | async-done | bytes 2097168
  151.1 1.7 select_bitcast_fusion
  152.8 3.4 collective-permute-start
  156.2 11.8 %collective-permute-done = f32[256,256]{1,0:T(8,128)S(1)} collective-permute-done((f32[256,256]{1,0:T(8,128)S(1)}, f32[256,256]{1,0:T(8,128)S(1)}, u32[]{:S(2)}, u32[]{:S(2)}) %collective-permute-start) | collective-permute-done | bytes 262176 | tf_op jit(solution)/shard_map/ppermute | solution.py:330
  168.0 1.7 bitcast_select_fusion
  169.7 0.7 pad_maximum_fusion.1
  170.4 0.0 copy-start.8
  170.4 1.7 fusion.3
  172.2 0.0 reduce-scatter.8.cloned.1.call-update
  172.2 0.0 copy-done.8
  172.2 0.0 reduce-scatter.6.cloned.1.call-done
  172.2 1.7 multiply_bitcast_fusion
  173.9 215.2 %reduce-scatter.8.cloned.1.call-done = f32[64,128]{1,0:T(8,128)} async-done(((f32[2048,128]{1,0:T(8,128)}), f32[64,128]{1,0:T(8,128)}) %reduce-scatter.8.cloned.1.call-update) | async-done | bytes 32784 | tf_op jit(solution)/shard_map/reduce_scatter | solution.py:336
  (3 shorter events, 0.0 us)
Async XLA Ops:
  8.0 143.1 %all-reduce.3.cloned.1.call-start = ((), (), s32[]{:S(2)}) async-start(), calls=%async_computation.4 | async-start | bytes 4194304
  13.9 1.0 copy-start
  14.9 0.9 copy-start.1
  15.9 0.9 copy-start.2
  55.5 1.3 copy-start.3
  56.8 0.8 copy-start.4
  57.7 0.8 copy-start.5
  58.5 0.7 copy-start.6
  87.1 1.5 copy-start.7
  90.1 0.7 copy-start.9
  90.1 82.1 %reduce-scatter.6.cloned.1.call-start = ((), (), s32[]{:S(2)}) async-start(), calls=%async_computation.2 | async-start | bytes 2359296 | tf_op jit(solution)/shard_map/reduce_scatter | solution.py:325
  90.7 298.4 %reduce-scatter.8.cloned.1.call-start = ((), (), s32[]{:S(2)}) async-start(), calls=%async_computation.3 | async-start | bytes 1081344 | tf_op jit(solution)/shard_map/reduce_scatter | solution.py:336
  152.8 15.2 %collective-permute-start = (f32[256,256]{1,0:T(8,128)S(1)}, f32[256,256]{1,0:T(8,128)S(1)}, u32[]{:S(2)}, u32[]{:S(2)}) collective-permute-start(f32[256,256]{1,0:T(8,128)S(1)} %select_bitcast_fusion), channel_id=1, source_target_pairs={{0,224},{32,192},{64,160},{96,128},{128,96},{160,64},{192,32},{224... | collective-permute-start | bytes 786440 | tf_op jit(solution)/shard_map/ppermute | solution.py:330
  170.4 1.8 copy-start.8
Sparse Core Ops, SparseCore 0:
  90.3 60.7 all-reduce.2
Sparse Core Ops, SparseCore 1:
  93.2 39.4 reduce-scatter.5
  172.3 216.8 reduce-scatter.7

commit v3 on v2

--- a/solution.py
+++ b/solution.py
@@ -220,7 +220,7 @@
     )(queries, rows, latents, w_value, keys)
 
 
-def attention_kernel(place, query_ref, row_ref, key_ref, value_ref, dq_ref, dk_ref, dv_ref, *, key_len, tok_len):
+def attention_kernel(place, query_ref, row_ref, key_ref, value_ref, dq_out, dk_out, dv_out, dq_ref, dk_ref, dv_ref, *, key_len, tok_len):
     low, col, half = place[0], place[1], place[2]
     dq_ref[...] = jnp.zeros_like(dq_ref)
     dk_ref[...] = jnp.zeros_like(dk_ref)
@@ -279,6 +279,9 @@
         return carry
 
     lax.fori_loop(0, 9, one_step, 0)
+    dq_out[...] = dq_ref[...].astype(bf16)
+    dk_out[...] = dk_ref[...].astype(bf16)
+    dv_out[...] = dv_ref[...].astype(bf16)
 
 
 def attention(place, queries, rows, keys, values):
@@ -286,16 +289,180 @@
     return pl.pallas_call(
         functools.partial(attention_kernel, key_len=512, tok_len=256),
         out_shape=(
-            jax.ShapeDtypeStruct((8, 512, 128), f32),
-            jax.ShapeDtypeStruct((2, 1024, 128), f32),
-            jax.ShapeDtypeStruct((2, 1024, 128), f32),
+            jax.ShapeDtypeStruct((8, 512, 128), bf16),
+            jax.ShapeDtypeStruct((2, 1024, 128), bf16),
+            jax.ShapeDtypeStruct((2, 1024, 128), bf16),
         ),
         in_specs=[pl.BlockSpec(memory_space=pltpu.SMEM), vmem, vmem, vmem, vmem],
         out_specs=[vmem, vmem, vmem],
+        scratch_shapes=[
+            pltpu.VMEM((8, 512, 128), f32),
+            pltpu.VMEM((2, 1024, 128), f32),
+            pltpu.VMEM((2, 1024, 128), f32),
+        ],
         compiler_params=pltpu.CompilerParams(vmem_limit_bytes=60 * 1024 * 1024),
         cost_estimate=pl.CostEstimate(flops=9 * 1024 * 512 * 2048, bytes_accessed=8 << 20, transcendentals=0),
         name="attention",
     )(place, queries, rows, keys, values)
+
+
+def scatter_kernel(
+    dq_ref, dk_ref, dv_ref, latent_ref, dq_out, dk_out, dv_out, weight_out,
+    dq_in, dq_stage, key_in, key_stage, mirror_stage, mirror_in, value_narrow,
+    weight_stage, weight_in, weight_pass, weight_mine, weight_last, send_sems, recv_sems,
+):
+    z, x = lax.axis_index("z"), lax.axis_index("x")
+    others = [{"z": lax.rem(z + hops, 8)} for hops in range(1, 8)]
+    up, down, mirror = others[0], others[6], {"z": 7 - z}
+    right, left = {"x": lax.rem(x + 1, 4)}, {"x": lax.rem(x + 3, 4)}
+    greet(others + [right, left])
+    sender = Sender(send_sems, recv_sems)
+    start, arrived = sender.start, sender.arrived
+    group = jnp.where(z < 4, 0, 1)
+    rows = (pl.ds(0, 256), pl.ds(256, 256))
+
+    def send_query(way, hops, part):
+        number = 0 if way == "up" else 1
+        device, sign = (up, 1) if way == "up" else (down, -1)
+        source = dq_ref.at[lax.rem(z + sign * hops + 8, 8), rows[part]]
+        if not (hops == 4 or (hops == 3 and part != number)):
+            arrived((way, hops + 1, part))
+            stage = dq_stage.at[number, hops - 1, part]
+            stage[...] = (source[...].astype(f32) + dq_in[number, hops, part].astype(f32)).astype(bf16)
+            source = stage
+        start((way, hops, part), source, dq_in.at[number, hops - 1, part], device)
+
+    def send_column(name, way, hops, part, pieces, inbox, stages):
+        number = 0 if way == "right" else 1
+        device, sign = (right, 1) if way == "right" else (left, -1)
+        source = pieces(lax.rem(x + sign * hops + 4, 4), part)
+        if hops == 1 and part == number:
+            arrived((name, way, 2, part))
+            stage = stages.at[number]
+            stage[...] = (source[...].astype(f32) + inbox[number, 2].astype(f32)).astype(bf16)
+            source = stage
+        slot = 2 if hops == 2 else part
+        start((name, way, hops, part), source, inbox.at[number, slot], device)
+
+    def column_sum(name, part, pieces, inbox):
+        arrived((name, "right", 1, part))
+        arrived((name, "left", 1, part))
+        return (
+            pieces(x, part)[...].astype(f32) + inbox[0, part].astype(f32) + inbox[1, part].astype(f32)
+        )
+
+    def first_columns(name, *args):
+        send_column(name, "right", 2, 0, *args)
+        send_column(name, "left", 2, 1, *args)
+        send_column(name, "right", 1, 1, *args)
+        send_column(name, "left", 1, 0, *args)
+
+    def last_columns(name, *args):
+        send_column(name, "right", 1, 0, *args)
+        send_column(name, "left", 1, 1, *args)
+
+    value_args = (lambda j, part: dv_ref.at[part, j]), key_in.at[0], key_stage.at[0]
+    key_args = (lambda j, part: dk_ref.at[part, j]), key_in.at[1], key_stage.at[1]
+    weight_args = (lambda j, part: weight_stage.at[j, pl.ds(4 * part, 4)]), weight_in, weight_pass
+
+    def own_rows(name, number, args, out):
+        sums = [column_sum(name, part, args[0], args[1]) for part in (0, 1)]
+        upper = z >= 4
+        mirror_stage[number] = jnp.where(upper, sums[0], sums[1]).astype(bf16)
+        out[group] = jnp.where(upper, sums[1], sums[0])
+        start((name, "mirror"), mirror_stage.at[number], mirror_in.at[number], mirror)
+
+    first_columns("value", *value_args)
+    send_query("up", 4, 0)
+    send_query("down", 4, 1)
+    send_query("up", 3, 1)
+    send_query("down", 3, 0)
+    first_columns("key", *key_args)
+    last_columns("value", *value_args)
+    send_query("up", 3, 0)
+    send_query("down", 3, 1)
+    own_rows("value", 0, value_args, dv_out)
+    last_columns("key", *key_args)
+    send_query("up", 2, 1)
+    send_query("down", 2, 0)
+    value_narrow[group] = dv_out[group].astype(bf16)
+    arrived(("value", "mirror"))
+    value_narrow[1 - group] = mirror_in[0]
+    dv_out[1 - group] = mirror_in[0].astype(f32)
+    narrow = value_narrow[...].reshape(512, 128)
+    for block in range(8):
+        part = lax.dot_general(latent_ref[block], narrow, cols_by_cols, preferred_element_type=f32)
+        weight_stage[:, block] = part.astype(bf16).reshape(4, 64, 128)
+        if block == 3:
+            send_column("weight", "right", 2, 0, *weight_args)
+            send_column("weight", "left", 1, 0, *weight_args)
+    send_column("weight", "left", 2, 1, *weight_args)
+    send_column("weight", "right", 1, 1, *weight_args)
+    send_query("up", 2, 0)
+    send_query("down", 2, 1)
+    send_query("up", 1, 1)
+    send_query("down", 1, 0)
+    last_columns("weight", *weight_args)
+    own_rows("key", 1, key_args, dk_out)
+    send_query("up", 1, 0)
+    send_query("down", 1, 1)
+    for part in (0, 1):
+        weight_mine[pl.ds(4 * part, 4)] = column_sum("weight", part, *weight_args[:2]).astype(bf16)
+    for hops in range(1, 8):
+        start(("weight", hops), weight_mine.at[lax.rem(z + hops, 8)], weight_last.at[hops - 1], others[hops - 1])
+    for part in (0, 1):
+        arrived(("up", 1, part))
+        arrived(("down", 1, part))
+        dq_out[rows[part]] = 0.125 * (
+            dq_ref[z, rows[part]].astype(f32)
+            + dq_in[0, 0, part].astype(f32)
+            + dq_in[1, 0, part].astype(f32)
+        )
+    arrived(("key", "mirror"))
+    dk_out[group] = 0.125 * dk_out[group]
+    dk_out[1 - group] = 0.125 * mirror_in[1].astype(f32)
+    total = weight_mine[z].astype(f32)
+    for hops in range(1, 8):
+        arrived(("weight", hops))
+        total += weight_last[hops - 1].astype(f32)
+    weight_out[...] = total
+    sender.finish()
+
+
+def scatter(dq, dk, dv, latents):
+    vmem = pl.BlockSpec(memory_space=pltpu.VMEM)
+    piece = (256, 128)
+    return pl.pallas_call(
+        scatter_kernel,
+        out_shape=(
+            jax.ShapeDtypeStruct((512, 128), f32),
+            jax.ShapeDtypeStruct((2, 256, 128), f32),
+            jax.ShapeDtypeStruct((2, 256, 128), f32),
+            jax.ShapeDtypeStruct((64, 128), f32),
+        ),
+        in_specs=[vmem] * 4,
+        out_specs=[vmem] * 4,
+        scratch_shapes=[
+            pltpu.VMEM((2, 4, 2, *piece), bf16),
+            pltpu.VMEM((2, 3, 2, *piece), bf16),
+            pltpu.VMEM((2, 2, 3, *piece), bf16),
+            pltpu.VMEM((2, 2, *piece), bf16),
+            pltpu.VMEM((2, *piece), bf16),
+            pltpu.VMEM((2, *piece), bf16),
+            pltpu.VMEM((2, *piece), bf16),
+            pltpu.VMEM((4, 8, 64, 128), bf16),
+            pltpu.VMEM((2, 3, 4, 64, 128), bf16),
+            pltpu.VMEM((2, 4, 64, 128), bf16),
+            pltpu.VMEM((8, 64, 128), bf16),
+            pltpu.VMEM((7, 64, 128), bf16),
+            pltpu.SemaphoreType.DMA((48,)),
+            pltpu.SemaphoreType.DMA((48,)),
+        ],
+        compiler_params=pltpu.CompilerParams(
+            collective_id=1, has_side_effects=True, vmem_limit_bytes=40 * 1024 * 1024
+        ),
+        name="scatter",
+    )(dq, dk, dv, latents)
 
 
 def per_device(queries, key_vectors, latents, w_value, log_sums, out_pair, cotangent, lambdas, out_gain):
@@ -303,7 +470,6 @@
     lam = lambdas[0]
     low = jnp.minimum(z, 7 - z)
     half = jnp.where(z < 4, 0, 1)
-    mirror = [(i, 7 - i) for i in range(8)]
 
     out_grad, first_term, second_term = head_cotangent(out_pair, cotangent, lam, out_gain)
     rows = jnp.stack(
@@ -316,25 +482,15 @@
         w_value.reshape(8, 256, 128),
         key_vectors.reshape(2, 256, 128),
     )
-    upper = z >= 4
     place = jnp.stack([low, x, half]).astype(jnp.int32)
     dq, dk, dv = attention(
         place, query_all, row_all, key_all.reshape(2, 1024, 128), value_all.reshape(2, 1024, 128)
     )
 
-    query_grad = lax.psum_scatter(dq, "z", scatter_dimension=0) * 0.125
-    both = jnp.concatenate([dk * 0.125, dv], axis=-1).reshape(2, 4, 256, 256)
-    own = lax.psum_scatter(both, "x", scatter_dimension=1)
-    kept = jnp.where(upper, own[1], own[0])
-    given = jnp.where(upper, own[0], own[1])
-    came = lax.ppermute(given, "z", mirror)
-    whole = jnp.concatenate([jnp.where(upper, came, kept), jnp.where(upper, kept, came)])
-    key_grad, value_grad = whole[:, :128], whole[:, 128:]
-    partial = lax.dot_general(
-        latent_all, value_grad.astype(bf16), (((1,), (0,)), ((), ())), preferred_element_type=f32
-    ).reshape(2048, 128)
-    weight_grad = lax.psum_scatter(partial, ("z", "x"), scatter_dimension=0, tiled=True)
-    return query_grad, key_grad, value_grad, weight_grad
+    query_grad, key_grad, value_grad, weight_grad = scatter(
+        dq, dk.reshape(2, 4, 256, 128), dv.reshape(2, 4, 256, 128), latent_all
+    )
+    return query_grad, key_grad.reshape(512, 128), value_grad.reshape(512, 128), weight_grad
 
 
 def solution(mesh):

time: 397 us -> 117 us (0.29)
  waiting for transfers between devices: 287 us -> 0 us
  Pallas kernels: 66.8 us -> 96.2 us
  between operations: 16.3 us -> 1.39 us
  other arithmetic: 13.8 us -> 5.06 us
  local copies, waits for them, and re-layouts: 7.24 us -> 12.5 us
    reduce_scatter x2 -> x0, waiting for transfers between devices: 215 us -> none  [the longest x1 215 us: per_device(): lax.psum_scatter(partial, ('z', 'x'), scatter_dimension=0, tiled=True)]
    unnamed x4 -> x0, waiting for transfers between devices: 60.3 us -> none
    pallas_call x0 -> x1, Pallas kernels: none -> 30 us  [scatter(): pl.pallas_call(scatter_kernel, out_shape=(jax.ShapeDtypeStruct((512, 128)...]
    ppermute x1 -> x0, waiting for transfers between devices: 11.8 us -> none  [per_device(): came = lax.ppermute(given, 'z', mirror)]
    unnamed x21 -> x24, local copies, waits for them, and re-layouts: 7.21 us -> 12.5 us
  transfers between devices with their start and end apart: 4 -> 0, of which waited for: 3 -> 0; matrix products, arithmetic and copies ran while one was open for 2% -> 0% of each run, Pallas kernels for 0% -> 0%
where the time goes in v3:
time: 117 us; the launch traced here: 115 us
  Pallas kernels  96.2 us (82%)
  local copies, waits for them, and re-layouts  12.5 us (11%)
  other arithmetic  5.06 us (4%)
  between operations  1.39 us (1%)
    pallas_call x1, Pallas kernels, gather(): pl.pallas_call(gather_kernel, out_shape=(jax.ShapeDtypeStruct((8, 512, 25...  38.8 us
    pallas_call x1, Pallas kernels, scatter(): pl.pallas_call(scatter_kernel, out_shape=(jax.ShapeDtypeStruct((512, 128)...  30 us
    pallas_call x1, Pallas kernels, attention(): pl.pallas_call(functools.partial(attention_kernel, key_len=512, tok_len=2...  27.4 us
    unnamed x24, local copies, waits for them, and re-layouts  12.5 us

profile of v3, /device:TPU:8, one launch (start us, length us, event | category | flops | bytes accessed | tf_op | source)
XLA Modules:
  0.0 115.2 jit_solution(10620449346479527604)
XLA Ops:
  1.3 0.6 pad_add_fusion.place
  1.9 0.8 subtract_bitcast_fusion
  2.7 1.3 %multiply_reduce_fusion.1 = (f32[512]{0:T(512)S(1)}, f32[512]{0:T(512)S(1)}) fusion(f32[]{:T(128)} %bitcast.18, bf16[512,256]{1,0:T(8,128)(2,1)} %param.14, f32[128]{0:T(128)} %param.17, bf16[512,128]{1,0:T(8,128)(2,1)} %param.15), kind=kLoop, calls=%fused_computation.10 | loop fusion | flops 654336 | bytes 397828 | tf_op jit(solution)/shard_map/reduce_sum | solution.py:25
  4.0 1.5 %fusion.1 = (f32[512]{0:T(512)S(1)}, f32[512]{0:T(512)S(1)}, bf16[512,128]{1,0:T(8,128)(2,1)S(1)}) fusion(bf16[512,256]{1,0:T(8,128)(2,1)} %param.14, f32[512]{0:T(512)S(1)} %get-tuple-element.37, f32[512]{0:T(512)S(1)} %get-tuple-element.36, f32[]{:T(128)} %bitcast.20, f32[128]{0:T(128)} %param.17, bf16[512,128]{1,0:T(8,128)(2,1)} %param.15, ...), kind=kLoop, calls=%fused_computation.5 | loop fusion | flops 1047552 | bytes 535044 | tf_op jit(solution)/shard_map/reduce_sum | solution.py:30
  5.5 0.9 pad_maximum_fusion.query_ref
  6.4 0.0 copy-start.1
  6.5 1.0 copy-done.1
  7.5 0.0 copy-start.4
  7.5 0.9 copy-done.4
  8.4 0.0 copy-start.5
  8.4 0.9 copy-done.5
  9.3 38.8 %gather.1 = (bf16[8,512,256]{2,1,0:T(8,128)(2,1)S(1)}, f32[8,8,512]{2,1,0:T(8,128)S(1)}, bf16[8,512,256]{2,1,0:T(8,128)(2,1)S(1)}, bf16[2,4,256,128]{3,2,1,0:T(8,128)(2,1)S(1)}, bf16[2,4,256,128]{3,2,1,0:T(8,128)(2,1)S(1)}) custom-call(bf16[512,256]{1,0:T(8,128)(2,1)S(1)} %pad_maximum_fusion.query_ref, f32[8,512]{1,0:T(8,128)S(1)} %concatenate.7.row_ref, ...), custom_call_target="tpu_custom_call" | custom-call | tf_op jit(solution)/shard_map/gather/pallas_call | solution.py:200
  48.1 0.0 copy-start.6
  48.1 1.3 %copy-done.6 = bf16[8,512,256]{2,1,0:T(8,128)(2,1)} copy-done((bf16[8,512,256]{2,1,0:T(8,128)(2,1)}, bf16[8,512,256]{2,1,0:T(8,128)(2,1)S(1)}, u32[]{:S(2)}) %copy-start.6) | copy-done | bytes 2097176
  49.5 0.0 copy-start.7
  49.5 0.8 copy-done.7
  50.3 0.0 copy-start.8
  50.3 0.8 copy-done.8
  51.1 0.0 copy-start.9
  51.1 0.7 copy-done.9
  51.7 27.4 %attention.1 = (bf16[8,512,128]{2,1,0:T(8,128)(2,1)}, bf16[2,1024,128]{2,1,0:T(8,128)(2,1)}, bf16[2,1024,128]{2,1,0:T(8,128)(2,1)}) custom-call(s32[3]{0:T(128)} %pad_add_fusion.place, bf16[8,512,256]{2,1,0:T(8,128)(2,1)} %copy-done.6, f32[8,8,512]{2,1,0:T(8,128)} %copy-done.9, bf16[2,1024,128]{2,1,0:T(8,128)(2,1)} %bitcast.27, bf16[2,1024,128]{2,1,0:T(8,128)(2,1)} %bitcast.28), custom_call_target="tpu_custom_call" | custom-call | flops 9663676416 | bytes 8388608 | tf_op jit(solution)/shard_map/attention/pallas_call | solution.py:289
  79.1 0.0 copy-start
  79.2 1.2 %copy-done = bf16[8,512,128]{2,1,0:T(8,128)(2,1)S(1)} copy-done((bf16[8,512,128]{2,1,0:T(8,128)(2,1)S(1)}, bf16[8,512,128]{2,1,0:T(8,128)(2,1)}, u32[]{:S(2)}) %copy-start) | copy-done | bytes 1048600
  80.4 0.0 copy-start.2
  80.4 1.0 copy-done.2
  81.4 0.0 copy-start.3
  81.4 1.0 copy-done.3
  82.5 30.0 %scatter.1 = (f32[512,128]{1,0:T(8,128)S(1)}, f32[2,256,128]{2,1,0:T(8,128)S(1)}, f32[2,256,128]{2,1,0:T(8,128)S(1)}, f32[64,128]{1,0:T(8,128)S(1)}) custom-call(bf16[8,512,128]{2,1,0:T(8,128)(2,1)S(1)} %copy-done, bf16[2,4,256,128]{3,2,1,0:T(8,128)(2,1)S(1)} %bitcast.22, bf16[2,4,256,128]{3,2,1,0:T(8,128)(2,1)S(1)} %bitcast.23, ...), custom_call_target="tpu_custom_call" | custom-call | tf_op jit(solution)/shard_map/scatter/pallas_call | solution.py:435
  112.5 0.7 copy.18
  113.2 0.7 copy.19
  113.9 0.7 copy.20
  114.6 0.6 copy.21
  (3 shorter events, 0.0 us)
Async XLA Ops:
  6.4 1.0 copy-start.1
  7.5 0.9 copy-start.4
  8.4 0.9 copy-start.5
  48.1 1.3 %copy-start.6 = (bf16[8,512,256]{2,1,0:T(8,128)(2,1)}, bf16[8,512,256]{2,1,0:T(8,128)(2,1)S(1)}, u32[]{:S(2)}) copy-start(bf16[8,512,256]{2,1,0:T(8,128)(2,1)S(1)} %get-tuple-element.16.query_ref) | copy-start | bytes 6291460
  49.5 0.8 copy-start.7
  50.3 0.8 copy-start.8
  51.1 0.7 copy-start.9
  79.1 1.2 %copy-start = (bf16[8,512,128]{2,1,0:T(8,128)(2,1)S(1)}, bf16[8,512,128]{2,1,0:T(8,128)(2,1)}, u32[]{:S(2)}) copy-start(bf16[8,512,128]{2,1,0:T(8,128)(2,1)} %get-tuple-element.20.dq_ref) | copy-start | bytes 3145732
  80.4 1.0 copy-start.2
  81.4 1.0 copy-start.3

commit v4 on v2

v4 whole, which is shorter than its diff:
```python
import functools
import math

import jax
import jax.numpy as jnp
from jax import lax
from jax.experimental import pallas as pl
from jax.experimental.pallas import tpu as pltpu
from jax.sharding import Mesh, PartitionSpec as P

norm_floor = 0.25
log2_e = math.log2(math.e)
f32 = jnp.float32
bf16 = jnp.bfloat16
rows_by_rows = (((1,), (1,)), ((), ()))
rows_by_cols = (((1,), (0,)), ((), ()))
cols_by_cols = (((0,), (0,)), ((), ()))
mesh_ids = pl.DeviceIdType.MESH
key_len, tok_len = 512, 256


class Sender:
    def __init__(self, send_sems, recv_sems):
        self.send_sems, self.recv_sems, self.copies = send_sems, recv_sems, {}

    def start(self, name, source, target, device):
        place = len(self.copies)
        copy = pltpu.make_async_remote_copy(
            src_ref=source,
            dst_ref=target,
            send_sem=self.send_sems.at[place],
            recv_sem=self.recv_sems.at[place],
            device_id=device,
            device_id_type=mesh_ids,
        )
        self.copies[name] = copy
        copy.start()

    def arrived(self, name):
        self.copies[name].wait_recv()

    def finish(self):
        for copy in self.copies.values():
            copy.wait_send()


def greet(devices):
    barrier = pltpu.get_barrier_semaphore()
    for device in devices:
        pl.semaphore_signal(barrier, inc=1, device_id=device, device_id_type=mesh_ids)
    pl.semaphore_wait(barrier, len(devices))


def turned(index, step, size):
    return lax.rem(index + (step + size), size)


def whole_kernel(
    query_hbm, key_hbm, latent_hbm, weight_hbm, log_hbm, pair_hbm, cotangent_hbm, gain_hbm, lam_ref,
    dq_out, dk_out, dv_out, weight_out,
    query_all, row_all, latent_all, key_all, value_all,
    key_given, weight_ref, log_ref, pair_ref, cotangent_ref, gain_ref, value_own,
    dq_acc, dk_acc, dv_acc, dq_in, dq_stage, column_in, column_stage,
    mirror_stage, mirror_in, value_narrow,
    weight_part, weight_stage, weight_in, weight_mine, weight_last,
    local_sems, send_sems, recv_sems,
):
    z, x, y, core = (lax.axis_index(name) for name in ("z", "x", "y", "core"))
    group = jnp.where(z < 4, 0, 1)
    half = group
    own_slot = y * 2 + core

    loads = {}
    for place, (name, source, target) in enumerate(
        (
            ("latent", latent_hbm, latent_all.at[own_slot]),
            ("key", key_hbm.at[half], key_all.at[group, x]),
            ("given", key_hbm.at[1 - half], key_given),
            ("pair", pair_hbm, pair_ref),
            ("cotangent", cotangent_hbm, cotangent_ref),
            ("gain", gain_hbm, gain_ref),
            ("log", log_hbm, log_ref),
            ("query", query_hbm, query_all.at[z, :, pl.ds(0, 128)]),
            ("weight", weight_hbm, weight_ref),
        )
    ):
        loads[name] = pltpu.make_async_copy(source, target, local_sems.at[place])
        loads[name].start()

    others = [{"z": turned(z, hops, 8)} for hops in range(1, 8)]
    up, down, mirror = others[0], others[6], {"z": 7 - z}
    right, left = {"x": turned(x, 1, 4)}, {"x": turned(x, -1, 4)}
    ahead, behind = {"y": turned(y, 1, 4)}, {"y": turned(y, -1, 4)}
    partner = {"core": 1 - core}
    greet(others + [right, left, ahead, behind, partner])
    sender = Sender(send_sems, recv_sems)
    start, arrived = sender.start, sender.arrived
    halves = (pl.ds(0, 256), pl.ds(256, 256))

    def latent_slot(step, part):
        return latent_all.at[turned(y, step, 4) * 2 + core, halves[part]]

    def latent_to_partner(step, part):
        start(("pair", step, part), latent_slot(step, part), latent_slot(step, part), partner)

    def send_query(way, hops, part):
        device, sign = (up, -1) if way == "up" else (down, 1)
        slot = query_all.at[turned(z, sign * hops, 8), halves[part]]
        start((way, hops, part), slot, slot, device)

    def send_rows(way, hops):
        device, sign = (up, -1) if way == "up" else (down, 1)
        slot = row_all.at[turned(z, sign * hops, 8)]
        start((way, hops, "rows"), slot, slot, device)

    def pass_query(hops, step):
        for way, part in (("up", step), ("down", 1 - step)):
            arrived((way, hops, part))
            if hops < 2 or (hops == 2 and step == 0):
                send_query(way, hops + 1, part)
            if step == 0 and hops < (4 if way == "up" else 3):
                arrived((way, hops, "rows"))
                if hops < (3 if way == "up" else 2):
                    send_rows(way, hops + 1)

    def open_share(name, given, target):
        slot = target.at[group, x]
        start((name, "mirror"), given, slot, mirror)
        start((name, "own", "right"), slot, slot, right)
        start((name, "own", "left"), slot, slot, left)

    def share_mirrored(name, target):
        arrived((name, "mirror"))
        slot = target.at[1 - group, x]
        start((name, "other", "left"), slot, slot, left)
        start((name, "other", "right"), slot, slot, right)

    def share_far(name, target):
        arrived((name, "own", "right"))
        slot = target.at[group, turned(x, -1, 4)]
        start((name, "own", "far"), slot, slot, right)
        arrived((name, "other", "left"))
        slot = target.at[1 - group, turned(x, 1, 4)]
        start((name, "other", "far"), slot, slot, left)

    def close_share(name):
        arrived((name, "own", "left"))
        arrived((name, "other", "right"))
        arrived((name, "own", "far"))
        arrived((name, "other", "far"))

    loads["latent"].wait()
    for way, part, device in (("ahead", 0, ahead), ("behind", 1, behind), ("ahead", 1, ahead), ("behind", 0, behind)):
        slot = latent_all.at[own_slot, halves[part]]
        start((way, part), slot, slot, device)
    start("pair", latent_all.at[own_slot], latent_all.at[own_slot], partner)
    loads["key"].wait()
    loads["given"].wait()
    open_share("key", key_given, key_all)

    for name in ("pair", "cotangent", "gain", "log", "query"):
        loads[name].wait()
    lam = lam_ref[0]
    first_out, second_out = pair_ref[:, 0:128].astype(f32), pair_ref[:, 128:256].astype(f32)
    merged = first_out - lam * second_out
    inv_norm = lax.rsqrt(jnp.mean(merged * merged, axis=-1, keepdims=True) + norm_floor)
    scaled = cotangent_ref[...].astype(f32) * gain_ref[...]
    inner_dot = jnp.mean(scaled * merged, axis=-1, keepdims=True)
    out_grad = (inv_norm * scaled - merged * (inv_norm * inv_norm * inv_norm) * inner_dot).astype(bf16)
    query_all[z, :, 128:256] = out_grad
    wide = out_grad.astype(f32)
    first_term = jnp.sum(wide * first_out, axis=-1, keepdims=True)
    second_term = jnp.sum(wide * second_out, axis=-1, keepdims=True)
    lane = lax.broadcasted_iota(jnp.int32, (1, 128), 1)
    terms = jnp.where(lane == 2, first_term, jnp.where(lane == 3, second_term, 0.0)).T[0:8]
    log_lam = jnp.log(jnp.full((1, 512), lam, f32)) * log2_e
    row_all[z] = terms
    row_all[z, 0:1, :] = log_ref[0:1, :] * log2_e
    row_all[z, 1:2, :] = log_ref[1:2, :] * log2_e - log_lam
    send_query("up", 0, 0)
    send_query("down", 0, 1)
    send_rows("up", 0)
    send_rows("down", 0)
    send_query("up", 0, 1)
    send_query("down", 0, 0)

    dq_acc[...] = jnp.zeros_like(dq_acc)
    dk_acc[...] = jnp.zeros_like(dk_acc)
    dv_acc[...] = jnp.zeros_like(dv_acc)

    arrived(("ahead", 0))
    start(("ahead", "far"), latent_slot(-1, 0), latent_slot(-1, 0), ahead)
    latent_to_partner(-1, 0)
    arrived(("behind", 1))
    start(("behind", "far"), latent_slot(1, 1), latent_slot(1, 1), behind)
    latent_to_partner(1, 1)
    share_mirrored("key", key_all)
    pass_query(0, 0)
    arrived(("ahead", 1))
    latent_to_partner(-1, 1)
    arrived(("behind", 0))
    latent_to_partner(1, 0)
    share_far("key", key_all)
    pass_query(0, 1)
    arrived(("ahead", "far"))
    latent_to_partner(2, 0)
    arrived(("behind", "far"))
    latent_to_partner(2, 1)
    arrived("pair")
    for step in (-1, 1, 2):
        for part in (0, 1):
            arrived(("pair", step, part))
    loads["weight"].wait()
    total = jnp.zeros((512, 128), f32)
    for slot in range(8):
        total += jnp.dot(latent_all[slot], weight_ref[slot], preferred_element_type=f32)
    value_own[...] = total.astype(bf16).reshape(2, 256, 128)
    value_all[group, x] = value_own[half]
    open_share("value", value_own.at[1 - half], value_all)
    pass_query(1, 0)
    share_mirrored("value", value_all)
    pass_query(1, 1)
    share_far("value", value_all)
    pass_query(2, 0)
    close_share("key")
    close_share("value")
    pass_query(2, 1)
    pass_query(3, 0)

    first_lanes = lane < 64

    def split(value):
        zero = jnp.zeros_like(value)
        return jnp.where(first_lanes, value, zero), jnp.where(first_lanes, zero, value)

    def tile(part, block, masked):
        for tok in range(0, 512, tok_len):
            toks = slice(tok, tok + tok_len)
            query, grad = query_all[block, toks, 0:128], query_all[block, toks, 128:256]
            query_0, query_1 = split(query)
            log_0, log_1 = row_all[block, 0:1, toks], row_all[block, 1:2, toks]
            term_0, term_1 = row_all[block, 2:3, toks], row_all[block, 3:4, toks]
            for key in range(0, 1024, key_len):
                cols = slice(key // 256, (key + key_len) // 256)
                key_0, key_1 = split(key_all[part, cols].reshape(key_len, 128))
                value = value_all[part, cols].reshape(key_len, 128)
                score_0 = lax.dot_general(key_0, query, rows_by_rows, preferred_element_type=f32)
                score_1 = lax.dot_general(key_1, query, rows_by_rows, preferred_element_type=f32)
                dot = lax.dot_general(value, grad, rows_by_rows, preferred_element_type=f32)
                map_0 = jnp.exp2(score_0 * (log2_e / 8) - log_0)
                map_1 = jnp.exp2(score_1 * (log2_e / 8) - log_1)
                if masked:
                    row = lax.broadcasted_iota(jnp.int32, (key_len, 1), 0) + key
                    key_pos = (row // 256 - x) * 512 + half * 256 + row % 256
                    tok_pos = lax.broadcasted_iota(jnp.int32, (1, tok_len), 1) + tok
                    visible = key_pos <= tok_pos
                    map_0 = jnp.where(visible, map_0, 0.0)
                    map_1 = jnp.where(visible, map_1, 0.0)
                grad_0 = (map_0 * (dot - term_0)).astype(bf16)
                grad_1 = (map_1 * (term_1 - dot)).astype(bf16)
                mixed = (map_0 - map_1).astype(bf16)
                dk = lax.dot_general(
                    grad_0, query_0, rows_by_cols, preferred_element_type=f32
                ) + lax.dot_general(grad_1, query_1, rows_by_cols, preferred_element_type=f32)
                dv = lax.dot_general(mixed, grad, rows_by_cols, preferred_element_type=f32)
                dk_acc[part, cols] += dk.reshape(key_len // 256, 256, 128)
                dv_acc[part, cols] += dv.reshape(key_len // 256, 256, 128)
                dq_acc[block, toks, :] += lax.dot_general(
                    grad_0, key_0, cols_by_cols, preferred_element_type=f32
                ) + lax.dot_general(grad_1, key_1, cols_by_cols, preferred_element_type=f32)

    def tiles(part, begin):
        def one(block, carry):
            tile(part, block, False)
            return carry

        lax.fori_loop(begin, 8, one, 0)

    def send_column(name, way, hops, part, pieces, inbox, stages):
        number = 0 if way == "right" else 1
        device, sign = (right, 1) if way == "right" else (left, -1)
        value = pieces(turned(x, sign * hops, 4), part)
        place = 0 if hops == 2 else 1
        if hops == 1 and part == number:
            arrived((name, way, 2, part))
            value += inbox[number, 2].astype(f32)
            place = 2
        stages[number, place] = value.astype(bf16)
        slot = 2 if hops == 2 else part
        start((name, way, hops, part), stages.at[number, place], inbox.at[number, slot], device)

    def first_columns(name, *args):
        send_column(name, "right", 2, 0, *args)
        send_column(name, "left", 2, 1, *args)
        send_column(name, "right", 1, 1, *args)
        send_column(name, "left", 1, 0, *args)

    def last_columns(name, *args):
        send_column(name, "right", 1, 0, *args)
        send_column(name, "left", 1, 1, *args)

    def column_sum(name, part, pieces, inbox):
        arrived((name, "right", 1, part))
        arrived((name, "left", 1, part))
        return pieces(x, part) + inbox[0, part].astype(f32) + inbox[1, part].astype(f32)

    def sum_args(acc, rows_of, number):
        def pieces(j, part):
            return acc[rows_of, j, 128 * part : 128 * part + 128, :]

        return pieces, column_in.at[number], column_stage.at[number]

    other_value, other_key = sum_args(dv_acc, 1 - group, 0), sum_args(dk_acc, 1 - group, 1)
    own_value, own_key = sum_args(dv_acc, group, 2), sum_args(dk_acc, group, 3)

    def mirrored_rows(name, number, args):
        for part in (0, 1):
            mirror_stage[number, 128 * part : 128 * part + 128] = column_sum(name, part, *args[:2]).astype(bf16)
        start((name, "mirror back"), mirror_stage.at[number], mirror_in.at[number], mirror)

    def own_rows(name, args, out):
        for part in (0, 1):
            out[group, 128 * part : 128 * part + 128] = column_sum(name, part, *args[:2])

    def send_dq(way, hops, part):
        number = 0 if way == "up" else 1
        device, sign = (up, 1) if way == "up" else (down, -1)
        value = dq_acc[turned(z, sign * hops, 8), halves[part]]
        if not (hops == 4 or (hops == 3 and part != number)):
            arrived(("dq", way, hops + 1, part))
            value += dq_in[number, hops, part].astype(f32)
        dq_stage[number, hops - 1, part] = value.astype(bf16)
        start(
            ("dq", way, hops, part),
            dq_stage.at[number, hops - 1, part],
            dq_in.at[number, hops - 1, part],
            device,
        )

    tile(1 - group, 7 - z, True)
    tiles(1 - group, 8 - z)
    first_columns("other value", *other_value)
    first_columns("other key", *other_key)
    tile(group, z, True)
    last_columns("other value", *other_value)
    last_columns("other key", *other_key)
    tiles(group, z + 1)
    first_columns("own value", *own_value)
    mirrored_rows("other value", 0, other_value)
    send_dq("up", 4, 0)
    send_dq("down", 4, 1)
    send_dq("up", 3, 1)
    send_dq("down", 3, 0)
    last_columns("own value", *own_value)
    first_columns("own key", *own_key)
    mirrored_rows("other key", 1, other_key)
    own_rows("own value", own_value, dv_out)
    value_narrow[group] = dv_out[group].astype(bf16)
    send_dq("up", 3, 0)
    send_dq("down", 3, 1)
    last_columns("own key", *own_key)
    arrived(("other value", "mirror back"))
    value_narrow[1 - group] = mirror_in[0]
    dv_out[1 - group] = mirror_in[0].astype(f32)

    weight_args = (lambda j, part: weight_part[j, 4 * part : 4 * part + 4]), weight_in, weight_stage
    narrow = value_narrow[...].reshape(512, 128)
    for block in range(8):
        part = lax.dot_general(latent_all[block], narrow, cols_by_cols, preferred_element_type=f32)
        weight_part[:, block] = part.reshape(4, 64, 128)
        if block == 3:
            send_column("weight", "right", 2, 0, *weight_args)
            send_column("weight", "left", 1, 0, *weight_args)
    send_column("weight", "left", 2, 1, *weight_args)
    send_column("weight", "right", 1, 1, *weight_args)
    send_dq("up", 2, 1)
    send_dq("down", 2, 0)
    own_rows("own key", own_key, dk_out)
    send_dq("up", 2, 0)
    send_dq("down", 2, 1)
    last_columns("weight", *weight_args)
    send_dq("up", 1, 1)
    send_dq("down", 1, 0)
    for part in (0, 1):
        weight_mine[4 * part : 4 * part + 4] = column_sum("weight", part, *weight_args[:2]).astype(bf16)
    for hops in range(1, 8):
        start(("weight", hops), weight_mine.at[turned(z, hops, 8)], weight_last.at[hops - 1], others[hops - 1])
    send_dq("up", 1, 0)
    send_dq("down", 1, 1)
    arrived(("other key", "mirror back"))
    dk_out[group] = 0.125 * dk_out[group]
    dk_out[1 - group] = 0.125 * mirror_in[1].astype(f32)
    for part in (0, 1):
        arrived(("dq", "up", 1, part))
        arrived(("dq", "down", 1, part))
        dq_out[halves[part]] = 0.125 * (
            dq_acc[z, halves[part]] + dq_in[0, 0, part].astype(f32) + dq_in[1, 0, part].astype(f32)
        )
    total = weight_mine[z].astype(f32)
    for hops in range(1, 8):
        arrived(("weight", hops))
        total += weight_last[hops - 1].astype(f32)
    weight_out[...] = total
    sender.finish()


def per_device(queries, key_vectors, latents, w_value, log_sums, out_pair, cotangent, lambdas, out_gain):
    anywhere, vmem = pl.BlockSpec(memory_space=pl.ANY), pl.BlockSpec(memory_space=pltpu.VMEM)
    scratch = (
        ((8, 512, 256), bf16),
        ((8, 8, 512), f32),
        ((8, 512, 256), bf16),
        ((2, 4, 256, 128), bf16),
        ((2, 4, 256, 128), bf16),
        ((256, 128), bf16),
        ((8, 256, 128), bf16),
        ((2, 512), f32),
        ((512, 256), bf16),
        ((512, 128), bf16),
        ((1, 128), f32),
        ((2, 256, 128), bf16),
        ((8, 512, 128), f32),
        ((2, 4, 256, 128), f32),
        ((2, 4, 256, 128), f32),
        ((2, 4, 2, 256, 128), bf16),
        ((2, 4, 2, 256, 128), bf16),
        ((4, 2, 3, 128, 128), bf16),
        ((4, 2, 3, 128, 128), bf16),
        ((2, 256, 128), bf16),
        ((2, 256, 128), bf16),
        ((2, 256, 128), bf16),
        ((4, 8, 64, 128), f32),
        ((2, 3, 4, 64, 128), bf16),
        ((2, 3, 4, 64, 128), bf16),
        ((8, 64, 128), bf16),
        ((7, 64, 128), bf16),
    )
    query_grad, key_grad, value_grad, weight_grad = pl.pallas_call(
        whole_kernel,
        out_shape=(
            jax.ShapeDtypeStruct((512, 128), f32),
            jax.ShapeDtypeStruct((2, 256, 128), f32),
            jax.ShapeDtypeStruct((2, 256, 128), f32),
            jax.ShapeDtypeStruct((64, 128), f32),
        ),
        in_specs=[anywhere] * 8 + [pl.BlockSpec(memory_space=pltpu.SMEM)],
        out_specs=[vmem] * 4,
        scratch_shapes=[pltpu.VMEM(*entry) for entry in scratch]
        + [
            pltpu.SemaphoreType.DMA((9,)),
            pltpu.SemaphoreType.DMA((110,)),
            pltpu.SemaphoreType.DMA((110,)),
        ],
        compiler_params=pltpu.CompilerParams(
            collective_id=0, has_side_effects=True, vmem_limit_bytes=60 * 1024 * 1024
        ),
        name="whole",
    )(
        queries,
        key_vectors.reshape(2, 256, 128),
        latents,
        w_value.reshape(8, 256, 128),
        log_sums.T,
        out_pair,
        cotangent,
        out_gain.reshape(1, 128),
        lambdas,
    )
    return query_grad, key_grad.reshape(512, 128), value_grad.reshape(512, 128), weight_grad


def solution(mesh):
    grid = Mesh(mesh.devices.reshape(8, 4, 4, 2), ("z", "x", "y", "core"))
    sp, tp = ("z", "x"), ("y", "core")
    return jax.shard_map(
        per_device,
        mesh=grid,
        in_specs=(
            P(sp, tp),
            P(sp, tp),
            P(sp, tp),
            P(None, tp),
            P(sp, tp),
            P(sp, tp),
            P(sp, tp),
            P(tp),
            P(),
        ),
        out_specs=(P(sp, tp), P(sp, tp), P(sp, tp), P(sp, tp)),
        check_vma=False,
    )
```

time: 397 us -> 94.3 us (0.24)
  waiting for transfers between devices: 287 us -> 0 us
  Pallas kernels: 66.8 us -> 88.6 us
  between operations: 16.3 us -> 1.3 us
  other arithmetic: 13.8 us -> 0 us
    reduce_scatter x2 -> x0, waiting for transfers between devices: 215 us -> none  [the longest x1 215 us: per_device(): lax.psum_scatter(partial, ('z', 'x'), scatter_dimension=0, tiled=True)]
    unnamed x4 -> x0, waiting for transfers between devices: 60.3 us -> none
    pallas_call x2 -> x1, Pallas kernels: 66.8 us -> 88.6 us  [per_device(): pl.pallas_call(whole_kernel, out_shape=(jax.ShapeDtypeStruct((512, 128),...]
    ppermute x1 -> x0, waiting for transfers between devices: 11.8 us -> none  [per_device(): came = lax.ppermute(given, 'z', mirror)]
  transfers between devices with their start and end apart: 4 -> 0, of which waited for: 3 -> 0; matrix products, arithmetic and copies ran while one was open for 2% -> 0% of each run, Pallas kernels for 0% -> 0%
where the time goes in v4:
time: 94.3 us; the launch traced here: 94.1 us
  Pallas kernels  88.6 us (94%)
  local copies, waits for them, and re-layouts  4.13 us (4%)
  between operations  1.3 us (1%)
    pallas_call x1, Pallas kernels, per_device(): pl.pallas_call(whole_kernel, out_shape=(jax.ShapeDtypeStruct((512, 128),...  88.6 us
    unnamed x10, local copies, waits for them, and re-layouts  4.13 us

profile of v4, /device:TPU:8, one launch (start us, length us, event | category | flops | bytes accessed | tf_op | source)
XLA Modules:
  0.0 94.1 jit_solution(5812574274596277273)
XLA Ops:
  1.3 88.6 %whole.1 = (f32[512,128]{1,0:T(8,128)}, f32[2,256,128]{2,1,0:T(8,128)}, f32[2,256,128]{2,1,0:T(8,128)}, f32[64,128]{1,0:T(8,128)}) custom-call(bf16[512,128]{1,0:T(8,128)(2,1)} %query_hbm.1, bf16[2,256,128]{2,1,0:T(8,128)(2,1)} %bitcast.9, bf16[512,256]{1,0:T(8,128)(2,1)} %latent_hbm.1, bf16[8,256,128]{2,1,0:T(8,128)(2,1)} %bitcast.6, f32[2,512]{1,0:T(2,128)} %bitcast.10, ...), custom_call_target="tpu_custom_call" | custom-call | tf_op jit(solution)/shard_map/whole/pallas_call | solution.py:438
  89.9 0.0 copy-start.1
  89.9 1.7 %copy.18 = f32[512,128]{1,0:T(8,128)} copy(f32[512,128]{1,0:T(8,128)} %get-tuple-element.16) | data formatting | bytes 524288
  91.6 0.0 copy-done.1
  91.6 0.0 copy-start
  91.6 0.7 copy.19
  92.3 0.3 copy-done
  92.7 0.0 copy-start.2
  92.7 0.7 copy.20
  93.4 0.1 copy-done.2
  93.4 0.6 copy.21
Async XLA Ops:
  89.9 1.7 %copy-start.1 = (f32[2,256,128]{2,1,0:T(8,128)S(1)}, f32[2,256,128]{2,1,0:T(8,128)}, u32[]{:S(2)}) copy-start(f32[2,256,128]{2,1,0:T(8,128)} %get-tuple-element.9) | copy-start | bytes 786436
  91.6 1.0 %copy-start = (f32[2,256,128]{2,1,0:T(8,128)S(1)}, f32[2,256,128]{2,1,0:T(8,128)}, u32[]{:S(2)}) copy-start(f32[2,256,128]{2,1,0:T(8,128)} %get-tuple-element.10) | copy-start | bytes 786436
  92.7 0.8 copy-start.2

commit v5 on v4

--- a/solution.py
+++ b/solution.py
@@ -16,7 +16,7 @@
 rows_by_cols = (((1,), (0,)), ((), ()))
 cols_by_cols = (((0,), (0,)), ((), ()))
 mesh_ids = pl.DeviceIdType.MESH
-key_len, tok_len = 512, 256
+key_len, tok_len = 1024, 256
 
 
 class Sender:
@@ -97,11 +97,42 @@
     start, arrived = sender.start, sender.arrived
     halves = (pl.ds(0, 256), pl.ds(256, 256))
 
-    def latent_slot(step, part):
-        return latent_all.at[turned(y, step, 4) * 2 + core, halves[part]]
-
-    def latent_to_partner(step, part):
-        start(("pair", step, part), latent_slot(step, part), latent_slot(step, part), partner)
+    def latent_slot(step, toks, part=None):
+        slot = latent_all.at[turned(y, step, 4) * 2 + core, toks]
+        return slot if part is None else slot.at[:, pl.ds(128 * part, 128)]
+
+    def latent_to_partner(name, step, toks):
+        start(("pair", name, step), latent_slot(step, toks), latent_slot(step, toks), partner)
+
+    def open_latents(name, toks):
+        for way, part, device in (("ahead", 0, ahead), ("behind", 1, behind), ("ahead", 1, ahead), ("behind", 0, behind)):
+            slot = latent_slot(0, toks, part)
+            start((name, way, part), slot, slot, device)
+        latent_to_partner(name, 0, toks)
+
+    def latents_far(name, toks):
+        for way, step, part, device in (("ahead", -1, 0, ahead), ("behind", 1, 1, behind)):
+            arrived((name, way, part))
+            slot = latent_slot(step, toks, part)
+            start((name, way, "far"), slot, slot, device)
+
+    def latents_near(name, toks):
+        for way, step, part in (("ahead", -1, 1), ("behind", 1, 0)):
+            arrived((name, way, part))
+            latent_to_partner(name, step, toks)
+
+    def latents_last(name, toks):
+        arrived((name, "ahead", "far"))
+        arrived((name, "behind", "far"))
+        latent_to_partner(name, 2, toks)
+
+    def values_of(name, toks):
+        for step in (0, -1, 1, 2):
+            arrived(("pair", name, step))
+        total = jnp.zeros((256, 128), f32)
+        for slot in range(8):
+            total += jnp.dot(latent_all[slot, toks], weight_ref[slot], preferred_element_type=f32)
+        return total.astype(bf16)
 
     def send_query(way, hops, part):
         device, sign = (up, -1) if way == "up" else (down, 1)
@@ -125,7 +156,8 @@
 
     def open_share(name, given, target):
         slot = target.at[group, x]
-        start((name, "mirror"), given, slot, mirror)
+        if given is not None:
+            start((name, "mirror"), given, slot, mirror)
         start((name, "own", "right"), slot, slot, right)
         start((name, "own", "left"), slot, slot, left)
 
@@ -150,10 +182,7 @@
         arrived((name, "other", "far"))
 
     loads["latent"].wait()
-    for way, part, device in (("ahead", 0, ahead), ("behind", 1, behind), ("ahead", 1, ahead), ("behind", 0, behind)):
-        slot = latent_all.at[own_slot, halves[part]]
-        start((way, part), slot, slot, device)
-    start("pair", latent_all.at[own_slot], latent_all.at[own_slot], partner)
+    open_latents("given", 1 - half)
     loads["key"].wait()
     loads["given"].wait()
     open_share("key", key_given, key_all)
@@ -188,35 +217,22 @@
     dk_acc[...] = jnp.zeros_like(dk_acc)
     dv_acc[...] = jnp.zeros_like(dv_acc)
 
-    arrived(("ahead", 0))
-    start(("ahead", "far"), latent_slot(-1, 0), latent_slot(-1, 0), ahead)
-    latent_to_partner(-1, 0)
-    arrived(("behind", 1))
-    start(("behind", "far"), latent_slot(1, 1), latent_slot(1, 1), behind)
-    latent_to_partner(1, 1)
+    latents_far("given", 1 - half)
+    open_latents("own", half)
     share_mirrored("key", key_all)
+    latents_near("given", 1 - half)
+    latents_last("given", 1 - half)
+    loads["weight"].wait()
     pass_query(0, 0)
-    arrived(("ahead", 1))
-    latent_to_partner(-1, 1)
-    arrived(("behind", 0))
-    latent_to_partner(1, 0)
+    value_own[...] = values_of("given", 1 - half)
+    start(("value", "mirror"), value_own, value_all.at[group, x], mirror)
+    latents_far("own", half)
     share_far("key", key_all)
+    latents_near("own", half)
     pass_query(0, 1)
-    arrived(("ahead", "far"))
-    latent_to_partner(2, 0)
-    arrived(("behind", "far"))
-    latent_to_partner(2, 1)
-    arrived("pair")
-    for step in (-1, 1, 2):
-        for part in (0, 1):
-            arrived(("pair", step, part))
-    loads["weight"].wait()
-    total = jnp.zeros((512, 128), f32)
-    for slot in range(8):
-        total += jnp.dot(latent_all[slot], weight_ref[slot], preferred_element_type=f32)
-    value_own[...] = total.astype(bf16).reshape(2, 256, 128)
-    value_all[group, x] = value_own[half]
-    open_share("value", value_own.at[1 - half], value_all)
+    latents_last("own", half)
+    value_all[group, x] = values_of("own", half)
+    open_share("value", None, value_all)
     pass_query(1, 0)
     share_mirrored("value", value_all)
     pass_query(1, 1)
@@ -225,7 +241,6 @@
     close_share("key")
     close_share("value")
     pass_query(2, 1)
-    pass_query(3, 0)
 
     first_lanes = lane < 64
 
@@ -238,6 +253,7 @@
             toks = slice(tok, tok + tok_len)
             query, grad = query_all[block, toks, 0:128], query_all[block, toks, 128:256]
             query_0, query_1 = split(query)
+            dq = jnp.zeros((128, tok_len), f32)
             log_0, log_1 = row_all[block, 0:1, toks], row_all[block, 1:2, toks]
             term_0, term_1 = row_all[block, 2:3, toks], row_all[block, 3:4, toks]
             for key in range(0, 1024, key_len):
@@ -265,9 +281,10 @@
                 dv = lax.dot_general(mixed, grad, rows_by_cols, preferred_element_type=f32)
                 dk_acc[part, cols] += dk.reshape(key_len // 256, 256, 128)
                 dv_acc[part, cols] += dv.reshape(key_len // 256, 256, 128)
-                dq_acc[block, toks, :] += lax.dot_general(
-                    grad_0, key_0, cols_by_cols, preferred_element_type=f32
-                ) + lax.dot_general(grad_1, key_1, cols_by_cols, preferred_element_type=f32)
+                dq += lax.dot_general(
+                    key_0, grad_0, cols_by_cols, preferred_element_type=f32
+                ) + lax.dot_general(key_1, grad_1, cols_by_cols, preferred_element_type=f32)
+            dq_acc[block, toks, :] += dq.T
 
     def tiles(part, begin):
         def one(block, carry):
@@ -338,6 +355,7 @@
         )
 
     tile(1 - group, 7 - z, True)
+    pass_query(3, 0)
     tiles(1 - group, 8 - z)
     first_columns("other value", *other_value)
     first_columns("other key", *other_key)
@@ -366,7 +384,7 @@
     weight_args = (lambda j, part: weight_part[j, 4 * part : 4 * part + 4]), weight_in, weight_stage
     narrow = value_narrow[...].reshape(512, 128)
     for block in range(8):
-        part = lax.dot_general(latent_all[block], narrow, cols_by_cols, preferred_element_type=f32)
+        part = lax.dot_general(latent_all[block].reshape(512, 256), narrow, cols_by_cols, preferred_element_type=f32)
         weight_part[:, block] = part.reshape(4, 64, 128)
         if block == 3:
             send_column("weight", "right", 2, 0, *weight_args)
@@ -388,12 +406,11 @@
     send_dq("up", 1, 0)
     send_dq("down", 1, 1)
     arrived(("other key", "mirror back"))
-    dk_out[group] = 0.125 * dk_out[group]
-    dk_out[1 - group] = 0.125 * mirror_in[1].astype(f32)
+    dk_out[1 - group] = mirror_in[1].astype(f32)
     for part in (0, 1):
         arrived(("dq", "up", 1, part))
         arrived(("dq", "down", 1, part))
-        dq_out[halves[part]] = 0.125 * (
+        dq_out[halves[part]] = (
             dq_acc[z, halves[part]] + dq_in[0, 0, part].astype(f32) + dq_in[1, 0, part].astype(f32)
         )
     total = weight_mine[z].astype(f32)
@@ -404,12 +421,19 @@
     sender.finish()
 
 
+def finish_kernel(dq_ref, dk_ref, dv_ref, weight_ref, dq_out, dk_out, dv_out, weight_out):
+    dq_out[...] = 0.125 * dq_ref[...]
+    dk_out[...] = 0.125 * dk_ref[...]
+    dv_out[...] = dv_ref[...]
+    weight_out[...] = weight_ref[...]
+
+
 def per_device(queries, key_vectors, latents, w_value, log_sums, out_pair, cotangent, lambdas, out_gain):
     anywhere, vmem = pl.BlockSpec(memory_space=pl.ANY), pl.BlockSpec(memory_space=pltpu.VMEM)
     scratch = (
         ((8, 512, 256), bf16),
         ((8, 8, 512), f32),
-        ((8, 512, 256), bf16),
+        ((8, 2, 256, 256), bf16),
         ((2, 4, 256, 128), bf16),
         ((2, 4, 256, 128), bf16),
         ((256, 128), bf16),
@@ -418,7 +442,7 @@
         ((512, 256), bf16),
         ((512, 128), bf16),
         ((1, 128), f32),
-        ((2, 256, 128), bf16),
+        ((256, 128), bf16),
         ((8, 512, 128), f32),
         ((2, 4, 256, 128), f32),
         ((2, 4, 256, 128), f32),
@@ -435,7 +459,7 @@
         ((8, 64, 128), bf16),
         ((7, 64, 128), bf16),
     )
-    query_grad, key_grad, value_grad, weight_grad = pl.pallas_call(
+    sums = pl.pallas_call(
         whole_kernel,
         out_shape=(
             jax.ShapeDtypeStruct((512, 128), f32),
@@ -448,8 +472,8 @@
         scratch_shapes=[pltpu.VMEM(*entry) for entry in scratch]
         + [
             pltpu.SemaphoreType.DMA((9,)),
-            pltpu.SemaphoreType.DMA((110,)),
-            pltpu.SemaphoreType.DMA((110,)),
+            pltpu.SemaphoreType.DMA((116,)),
+            pltpu.SemaphoreType.DMA((116,)),
         ],
         compiler_params=pltpu.CompilerParams(
             collective_id=0, has_side_effects=True, vmem_limit_bytes=60 * 1024 * 1024
@@ -458,7 +482,7 @@
     )(
         queries,
         key_vectors.reshape(2, 256, 128),
-        latents,
+        latents.reshape(2, 256, 256),
         w_value.reshape(8, 256, 128),
         log_sums.T,
         out_pair,
@@ -466,6 +490,14 @@
         out_gain.reshape(1, 128),
         lambdas,
     )
+    query_grad, key_grad, value_grad, weight_grad = pl.pallas_call(
+        finish_kernel,
+        out_shape=tuple(jax.ShapeDtypeStruct(part.shape, f32) for part in sums),
+        in_specs=[vmem] * 4,
+        out_specs=[vmem] * 4,
+        compiler_params=pltpu.CompilerParams(vmem_limit_bytes=8 * 1024 * 1024),
+        name="finish",
+    )(*sums)
     return query_grad, key_grad.reshape(512, 128), value_grad.reshape(512, 128), weight_grad
 
 

time: 94.3 us -> 89.7 us (0.951)
  Pallas kernels: 88.6 us -> 84 us
    pallas_call x1, Pallas kernels: 88.6 us -> 83.1 us  [per_device(): pl.pallas_call(whole_kernel, out_shape=(jax.ShapeDtypeStruct((512, 128),...]
    unnamed x10 -> x8, local copies, waits for them, and re-layouts: 4.13 us -> 3.6 us
where the time goes in v5:
time: 89.7 us; the launch traced here: 88.9 us
  Pallas kernels  84 us (94%)
  local copies, waits for them, and re-layouts  3.6 us (4%)
  between operations  1.3 us (1%)
    pallas_call x1, Pallas kernels, per_device(): pl.pallas_call(whole_kernel, out_shape=(jax.ShapeDtypeStruct((512, 128),...  83.1 us
    unnamed x8, local copies, waits for them, and re-layouts  3.6 us

profile of v5, /device:TPU:8, one launch (start us, length us, event | category | flops | bytes accessed | tf_op | source)
XLA Modules:
  0.0 88.9 jit_solution(15550862581028145284)
XLA Ops:
  1.3 83.1 %whole.1 = (f32[512,128]{1,0:T(8,128)}, f32[2,256,128]{2,1,0:T(8,128)}, f32[2,256,128]{2,1,0:T(8,128)}, f32[64,128]{1,0:T(8,128)}) custom-call(bf16[512,128]{1,0:T(8,128)(2,1)} %query_hbm.1, bf16[2,256,128]{2,1,0:T(8,128)(2,1)} %bitcast.9, bf16[2,256,256]{2,1,0:T(8,128)(2,1)} %bitcast.8, bf16[8,256,128]{2,1,0:T(8,128)(2,1)} %bitcast.7, f32[2,512]{1,0:T(2,128)} %bitcast.10, ...), custom_call_target="tpu_custom_call" | custom-call | tf_op jit(solution)/shard_map/whole/pallas_call | solution.py:462
  84.4 0.0 copy-start
  84.4 0.9 %copy-done = f32[512,128]{1,0:T(8,128)S(1)} copy-done((f32[512,128]{1,0:T(8,128)S(1)}, f32[512,128]{1,0:T(8,128)}, u32[]{:S(2)}) %copy-start) | copy-done | bytes 262168
  85.3 0.0 copy-start.1
  85.3 0.9 %copy-done.1 = f32[2,256,128]{2,1,0:T(8,128)S(1)} copy-done((f32[2,256,128]{2,1,0:T(8,128)S(1)}, f32[2,256,128]{2,1,0:T(8,128)}, u32[]{:S(2)}) %copy-start.1) | copy-done | bytes 262168
  86.3 0.0 copy-start.2
  86.3 0.9 %copy-done.2 = f32[2,256,128]{2,1,0:T(8,128)S(1)} copy-done((f32[2,256,128]{2,1,0:T(8,128)S(1)}, f32[2,256,128]{2,1,0:T(8,128)}, u32[]{:S(2)}) %copy-start.2) | copy-done | bytes 262168
  87.2 0.0 copy-start.3
  87.2 0.8 copy-done.3
  88.0 0.9 %finish.1 = (f32[512,128]{1,0:T(8,128)}, f32[2,256,128]{2,1,0:T(8,128)}, f32[2,256,128]{2,1,0:T(8,128)}, f32[64,128]{1,0:T(8,128)}) custom-call(f32[512,128]{1,0:T(8,128)S(1)} %copy-done, f32[2,256,128]{2,1,0:T(8,128)S(1)} %copy-done.1, f32[2,256,128]{2,1,0:T(8,128)S(1)} %copy-done.2, f32[64,128]{1,0:T(8,128)S(1)} %copy-done.3), custom_call_target="tpu_custom_call" | custom-call | tf_op jit(solution)/shard_map/finish/pallas_call | solution.py:493
Async XLA Ops:
  84.4 1.0 %copy-start = (f32[512,128]{1,0:T(8,128)S(1)}, f32[512,128]{1,0:T(8,128)}, u32[]{:S(2)}) copy-start(f32[512,128]{1,0:T(8,128)} %get-tuple-element.12.dq_ref) | copy-start | bytes 786436
  85.3 0.9 %copy-start.1 = (f32[2,256,128]{2,1,0:T(8,128)S(1)}, f32[2,256,128]{2,1,0:T(8,128)}, u32[]{:S(2)}) copy-start(f32[2,256,128]{2,1,0:T(8,128)} %get-tuple-element.13.dk_ref) | copy-start | bytes 786436
  86.3 0.9 %copy-start.2 = (f32[2,256,128]{2,1,0:T(8,128)S(1)}, f32[2,256,128]{2,1,0:T(8,128)}, u32[]{:S(2)}) copy-start(f32[2,256,128]{2,1,0:T(8,128)} %get-tuple-element.14.dv_ref) | copy-start | bytes 786436
  87.2 0.8 copy-start.3

commit v6 on v5

v6 whole, which is shorter than its diff:
```python
import functools
import math

import jax
import jax.numpy as jnp
from jax import lax
from jax.experimental import pallas as pl
from jax.experimental.pallas import tpu as pltpu
from jax.sharding import Mesh, PartitionSpec as P

norm_floor = 0.25
log2_e = math.log2(math.e)
f32 = jnp.float32
bf16 = jnp.bfloat16
rows_by_rows = (((1,), (1,)), ((), ()))
rows_by_cols = (((1,), (0,)), ((), ()))
cols_by_cols = (((0,), (0,)), ((), ()))
mesh_ids = pl.DeviceIdType.MESH
tok_len = 256


class Sender:
    def __init__(self, send_sems, recv_sems):
        self.send_sems, self.recv_sems = send_sems, recv_sems
        self.copies = {}

    def plan(self, name, source, target, device):
        place = len(self.copies)
        self.copies[name] = pltpu.make_async_remote_copy(
            src_ref=source,
            dst_ref=target,
            send_sem=self.send_sems.at[place],
            recv_sem=self.recv_sems.at[place],
            device_id=device,
            device_id_type=mesh_ids,
        )

    def start(self, name):
        self.copies[name].start()

    def arrived(self, name):
        self.copies[name].wait_recv()

    def finish(self):
        for copy in self.copies.values():
            copy.wait_send()


def greet(devices):
    barrier = pltpu.get_barrier_semaphore()
    for device in devices:
        pl.semaphore_signal(barrier, inc=1, device_id=device, device_id_type=mesh_ids)
    pl.semaphore_wait(barrier, len(devices))


def turned(index, step, size):
    return lax.rem(index + (step + size), size)


def whole_kernel(
    query_hbm, key_hbm, latent_hbm, weight_hbm, log_hbm, pair_hbm, cotangent_hbm, gain_hbm, lam_ref,
    dq_out, dk_out, dv_out, weight_out,
    query_all, grad_all, row_all, latent_all, key_all, value_all,
    maps, key_given, weight_ref, log_ref, pair_ref, cotangent_ref, gain_ref, value_own,
    dq_acc, dk_acc, dv_acc, dq_in, dq_stage, column_in, column_stage,
    mirror_stage, mirror_in, value_narrow,
    weight_part, weight_stage, weight_in, weight_mine, weight_last,
    local_sems, send_sems, recv_sems,
):
    z, x, y, core = (lax.axis_index(name) for name in ("z", "x", "y", "core"))
    group = jnp.where(z < 4, 0, 1)
    half = group
    own_slot = y * 2 + core

    loads = {}
    for place, (name, source, target) in enumerate(
        (
            ("latent", latent_hbm, latent_all.at[own_slot]),
            ("key", key_hbm.at[half], key_all.at[group, x]),
            ("given", key_hbm.at[1 - half], key_given),
            ("pair", pair_hbm, pair_ref),
            ("cotangent", cotangent_hbm, cotangent_ref),
            ("gain", gain_hbm, gain_ref),
            ("log", log_hbm, log_ref),
            ("query", query_hbm, query_all.at[z]),
            ("weight", weight_hbm, weight_ref),
        )
    ):
        loads[name] = pltpu.make_async_copy(source, target, local_sems.at[place])
        loads[name].start()

    others = [{"z": turned(z, hops, 8)} for hops in range(1, 8)]
    up, down, mirror = others[0], others[6], {"z": 7 - z}
    right, left = {"x": turned(x, 1, 4)}, {"x": turned(x, -1, 4)}
    ahead, behind = {"y": turned(y, 1, 4)}, {"y": turned(y, -1, 4)}
    partner = {"core": 1 - core}
    greet(others + [right, left, ahead, behind, partner])
    sender = Sender(send_sems, recv_sems)
    plan, start, arrived = sender.plan, sender.start, sender.arrived
    halves = (pl.ds(0, 256), pl.ds(256, 256))

    def latent_slot(step, toks, part=None):
        slot = latent_all.at[turned(y, step, 4) * 2 + core, toks]
        return slot if part is None else slot.at[:, pl.ds(128 * part, 128)]

    sides = {"ahead": (ahead, -1, 0), "behind": (behind, 1, 1)}
    for name, toks in (("given", 1 - half), ("own", half)):
        for way, (device, step, far) in sides.items():
            for part in (0, 1):
                plan((name, way, part), latent_slot(0, toks, part), latent_slot(0, toks, part), device)
            plan((name, way, "far"), latent_slot(step, toks, far), latent_slot(step, toks, far), device)
        for step in (0, -1, 1, 2):
            plan(("pair", name, step), latent_slot(step, toks), latent_slot(step, toks), partner)
    for way, device, sign in (("up", up, -1), ("down", down, 1)):
        for hops in range(4):
            index = turned(z, sign * hops, 8)
            for part in (0, 1):
                if hops < 3 or (way == "up") == (part == 0):
                    slot = (query_all, grad_all)[part].at[index]
                    plan((way, hops, part), slot, slot, device)
            if hops < 3 or way == "up":
                plan((way, hops, "rows"), row_all.at[index], row_all.at[index], device)
    for name, given, target in (("key", key_given, key_all), ("value", value_own, value_all)):
        own, other = target.at[group, x], target.at[1 - group, x]
        plan((name, "mirror"), given, own, mirror)
        for way, device, step in (("right", right, -1), ("left", left, 1)):
            plan((name, "own", way), own, own, device)
            plan((name, "other", way), other, other, device)
        own, other = target.at[group, turned(x, -1, 4)], target.at[1 - group, turned(x, 1, 4)]
        plan((name, "own", "far"), own, own, right)
        plan((name, "other", "far"), other, other, left)
    for name, inbox, stages in (
        ("other value", column_in.at[0], column_stage.at[0]),
        ("own value", column_in.at[1], column_stage.at[1]),
        ("other key", column_in.at[2], column_stage.at[2]),
        ("own key", column_in.at[3], column_stage.at[3]),
        ("weight", weight_in, weight_stage),
    ):
        for number, (way, device) in enumerate((("right", right), ("left", left))):
            plan((name, way, 2, number), stages.at[number, 0], inbox.at[number, 2], device)
            plan((name, way, 1, 1 - number), stages.at[number, 1], inbox.at[number, 1 - number], device)
            plan((name, way, 1, number), stages.at[number, 2], inbox.at[number, number], device)
    for number in (0, 1):
        plan(("mirror back", number), mirror_stage.at[number], mirror_in.at[number], mirror)
    for number, (way, device) in enumerate((("up", up), ("down", down))):
        for hops in (4, 3, 2, 1):
            for part in (0, 1):
                if hops < 4 or part == number:
                    place = number, hops - 1, part
                    plan(("dq", way, hops, part), dq_stage.at[place], dq_in.at[place], device)
    for hops in range(1, 8):
        plan(("weight", hops), weight_mine.at[turned(z, hops, 8)], weight_last.at[hops - 1], others[hops - 1])

    def open_latents(name):
        for part in (0, 1):
            start((name, "ahead", part))
            start((name, "behind", 1 - part))
        start(("pair", name, 0))

    def latents_far(name):
        for way, (_, _, far) in sides.items():
            arrived((name, way, far))
            start((name, way, "far"))

    def latents_near(name):
        for way, (_, step, far) in sides.items():
            arrived((name, way, 1 - far))
            start(("pair", name, step))

    def latents_last(name):
        arrived((name, "ahead", "far"))
        arrived((name, "behind", "far"))
        start(("pair", name, 2))

    def values_of(name, toks):
        for step in (0, -1, 1, 2):
            arrived(("pair", name, step))
        total = jnp.zeros((256, 128), f32)
        for slot in range(8):
            total += jnp.dot(latent_all[slot, toks], weight_ref[slot], preferred_element_type=f32)
        return total.astype(bf16)

    def send_query(hops, part):
        for way in ("up", "down"):
            if (way, hops, part) in sender.copies:
                start((way, hops, part))
            if part == 1 and (way, hops, "rows") in sender.copies:
                start((way, hops, "rows"))

    def pass_query(hops, part):
        for way in ("up", "down"):
            if (way, hops, part) in sender.copies:
                arrived((way, hops, part))
                if (way, hops + 1, part) in sender.copies:
                    start((way, hops + 1, part))
            if part == 1 and (way, hops, "rows") in sender.copies:
                arrived((way, hops, "rows"))
                if (way, hops + 1, "rows") in sender.copies:
                    start((way, hops + 1, "rows"))

    def share_own(name):
        start((name, "own", "right"))
        start((name, "own", "left"))

    def share_mirrored(name):
        arrived((name, "mirror"))
        start((name, "other", "left"))
        start((name, "other", "right"))

    def share_far(name):
        arrived((name, "own", "right"))
        start((name, "own", "far"))
        arrived((name, "other", "left"))
        start((name, "other", "far"))

    def close_share(name):
        for which, way in (("own", "left"), ("other", "right"), ("own", "far"), ("other", "far")):
            arrived((name, which, way))

    loads["latent"].wait()
    open_latents("given")
    loads["key"].wait()
    loads["given"].wait()
    start(("key", "mirror"))
    share_own("key")
    loads["query"].wait()
    send_query(0, 0)

    for name in ("pair", "cotangent", "gain", "log"):
        loads[name].wait()
    lam = lam_ref[0]
    first_out, second_out = pair_ref[:, 0:128].astype(f32), pair_ref[:, 128:256].astype(f32)
    merged = first_out - lam * second_out
    inv_norm = lax.rsqrt(jnp.mean(merged * merged, axis=-1, keepdims=True) + norm_floor)
    scaled = cotangent_ref[...].astype(f32) * gain_ref[...]
    inner_dot = jnp.mean(scaled * merged, axis=-1, keepdims=True)
    out_grad = (inv_norm * scaled - merged * (inv_norm * inv_norm * inv_norm) * inner_dot).astype(bf16)
    grad_all[z] = out_grad
    wide = out_grad.astype(f32)
    first_term = jnp.sum(wide * first_out, axis=-1, keepdims=True)
    second_term = jnp.sum(wide * second_out, axis=-1, keepdims=True)
    lane = lax.broadcasted_iota(jnp.int32, (1, 128), 1)
    terms = jnp.where(lane == 0, first_term, second_term).T
    log_lam = jnp.log(jnp.full((1, 512), lam, f32)) * log2_e
    row_all[z, 2:4, :] = terms[0:2]
    row_all[z, 0:1, :] = log_ref[0:1, :] * log2_e
    row_all[z, 1:2, :] = log_ref[1:2, :] * log2_e - log_lam
    send_query(0, 1)

    dq_acc[...] = jnp.zeros_like(dq_acc)
    dk_acc[...] = jnp.zeros_like(dk_acc)
    dv_acc[...] = jnp.zeros_like(dv_acc)

    latents_far("given")
    open_latents("own")
    share_mirrored("key")
    latents_near("given")
    latents_last("given")
    loads["weight"].wait()
    pass_query(0, 0)
    value_own[...] = values_of("given", 1 - half)
    start(("value", "mirror"))
    share_far("key")
    latents_far("own")
    pass_query(0, 1)
    latents_near("own")
    close_share("key")

    first_lanes = lane < 64

    def split(value):
        zero = jnp.zeros_like(value)
        return jnp.where(first_lanes, value, zero), jnp.where(first_lanes, zero, value)

    def block_at(count):
        hops = (count + 1) // 2
        return turned(z, jnp.where(count % 2 == 1, -hops, hops), 8)

    def both_groups(block, work):
        def one(number, carry):
            own = number == 1
            part = jnp.where(own, group, 1 - group)
            row = jnp.where(own, z, 7 - z)
            slot = jnp.where(own, block + 1, block - 7 + z)
            pl.when(block >= row)(lambda: work(part, row, slot))
            return carry

        lax.fori_loop(0, 2, one, 0)

    def maps_tile(part, block, slot, masked):
        key_0, key_1 = split(key_all[part].reshape(1024, 128))
        for tok in range(0, 512, tok_len):
            toks = slice(tok, tok + tok_len)
            query, grad = query_all[block, toks], grad_all[block, toks]
            score_0 = lax.dot_general(key_0, query, rows_by_rows, preferred_element_type=f32)
            score_1 = lax.dot_general(key_1, query, rows_by_rows, preferred_element_type=f32)
            map_0 = jnp.exp2(score_0 * (log2_e / 8) - row_all[block, 0:1, toks])
            map_1 = jnp.exp2(score_1 * (log2_e / 8) - row_all[block, 1:2, toks])
            if masked:
                row = lax.broadcasted_iota(jnp.int32, (1024, 1), 0)
                key_pos = (row // 256 - x) * 512 + half * 256 + row % 256
                tok_pos = lax.broadcasted_iota(jnp.int32, (1, tok_len), 1) + tok
                visible = key_pos <= tok_pos
                map_0 = jnp.where(visible, map_0, 0.0)
                map_1 = jnp.where(visible, map_1, 0.0)
            maps[slot, 0, :, toks] = map_0.astype(bf16)
            maps[slot, 1, :, toks] = map_1.astype(bf16)
            mixed = (map_0 - map_1).astype(bf16)
            dv = lax.dot_general(mixed, grad, rows_by_cols, preferred_element_type=f32)
            dv_acc[part] += dv.reshape(4, 256, 128)

    def grads_tile(part, block, slot):
        key_0, key_1 = split(key_all[part].reshape(1024, 128))
        value = value_all[part].reshape(1024, 128)
        for tok in range(0, 512, tok_len):
            toks = slice(tok, tok + tok_len)
            query_0, query_1 = split(query_all[block, toks])
            dot = lax.dot_general(value, grad_all[block, toks], rows_by_rows, preferred_element_type=f32)
            map_0, map_1 = maps[slot, 0, :, toks].astype(f32), maps[slot, 1, :, toks].astype(f32)
            grad_0 = (map_0 * (dot - row_all[block, 2:3, toks])).astype(bf16)
            grad_1 = (map_1 * (row_all[block, 3:4, toks] - dot)).astype(bf16)
            dk = lax.dot_general(
                grad_0, query_0, rows_by_cols, preferred_element_type=f32
            ) + lax.dot_general(grad_1, query_1, rows_by_cols, preferred_element_type=f32)
            dk_acc[part] += dk.reshape(4, 256, 128)
            dq = lax.dot_general(
                key_0, grad_0, cols_by_cols, preferred_element_type=f32
            ) + lax.dot_general(key_1, grad_1, cols_by_cols, preferred_element_type=f32)
            dq_acc[block, toks, :] += dq.T

    def send_column(name, way, hops, part, pieces, inbox, stages):
        number, sign = (0, 1) if way == "right" else (1, -1)
        value = pieces(turned(x, sign * hops, 4), part)
        place = 0 if hops == 2 else 1
        if hops == 1 and part == number:
            arrived((name, way, 2, part))
            value += inbox[number, 2].astype(f32)
            place = 2
        stages[number, place] = value.astype(bf16)
        start((name, way, hops, part))

    def first_columns(name, *args):
        send_column(name, "right", 2, 0, *args)
        send_column(name, "left", 2, 1, *args)
        send_column(name, "right", 1, 1, *args)
        send_column(name, "left", 1, 0, *args)

    def last_columns(name, *args):
        send_column(name, "right", 1, 0, *args)
        send_column(name, "left", 1, 1, *args)

    def column_sum(name, part, pieces, inbox):
        arrived((name, "right", 1, part))
        arrived((name, "left", 1, part))
        return pieces(x, part) + inbox[0, part].astype(f32) + inbox[1, part].astype(f32)

    def sum_args(acc, rows_of, number):
        def pieces(j, part):
            return acc[rows_of, j, 128 * part : 128 * part + 128, :]

        return pieces, column_in.at[number], column_stage.at[number]

    other_value, own_value = sum_args(dv_acc, 1 - group, 0), sum_args(dv_acc, group, 1)
    other_key, own_key = sum_args(dk_acc, 1 - group, 2), sum_args(dk_acc, group, 3)
    weight_args = (lambda j, part: weight_part[j, 4 * part : 4 * part + 4]), weight_in, weight_stage

    def mirrored_rows(name, number, args):
        for part in (0, 1):
            mirror_stage[number, 128 * part : 128 * part + 128] = column_sum(name, part, *args[:2]).astype(bf16)
        start(("mirror back", number))

    def own_rows(name, args, out):
        for part in (0, 1):
            out[group, 128 * part : 128 * part + 128] = column_sum(name, part, *args[:2])

    def send_dq(way, hops):
        number, sign = (0, 1) if way == "up" else (1, -1)
        for part in (number, 1 - number):
            if hops == 4 and part != number:
                continue
            value = dq_acc[turned(z, sign * hops, 8), halves[part]]
            if hops < 3 or (hops == 3 and part == number):
                arrived(("dq", way, hops + 1, part))
                value += dq_in[number, hops, part].astype(f32)
            dq_stage[number, hops - 1, part] = value.astype(bf16)
            start(("dq", way, hops, part))

    def maps_step(count, carry):
        @pl.when(count == 1)
        def _():
            latents_last("own")
            value_all[group, x] = values_of("own", half)
            share_own("value")

        @pl.when(count == 2)
        def _():
            pass_query(1, 0)
            share_mirrored("value")

        @pl.when(count == 3)
        def _():
            pass_query(1, 1)
            share_far("value")

        pl.when(count == 4)(lambda: pass_query(2, 0))
        pl.when(count == 5)(lambda: pass_query(2, 1))

        @pl.when(count == 7)
        def _():
            pass_query(3, 0)
            pass_query(3, 1)

        block = block_at(count)

        def work(part, row, slot):
            pl.when(block == row)(lambda: maps_tile(part, block, slot, True))
            pl.when(block != row)(lambda: maps_tile(part, block, slot, False))

        both_groups(block, work)
        return carry

    lax.fori_loop(0, 8, maps_step, 0)
    first_columns("other value", *other_value)
    first_columns("own value", *own_value)
    close_share("value")

    def values_summed():
        mirrored_rows("other value", 0, other_value)
        own_rows("own value", own_value, dv_out)
        value_narrow[group] = dv_out[group].astype(bf16)

    def weights_made():
        arrived(("mirror back", 0))
        value_narrow[1 - group] = mirror_in[0]
        dv_out[1 - group] = mirror_in[0].astype(f32)
        narrow = value_narrow[...].reshape(512, 128)
        for block in range(8):
            part = lax.dot_general(
                latent_all[block].reshape(512, 256), narrow, cols_by_cols, preferred_element_type=f32
            )
            weight_part[:, block] = part.reshape(4, 64, 128)
            if block == 3:
                send_column("weight", "right", 2, 0, *weight_args)
                send_column("weight", "left", 1, 0, *weight_args)
        send_column("weight", "left", 2, 1, *weight_args)
        send_column("weight", "right", 1, 1, *weight_args)

    def weights_summed():
        for part in (0, 1):
            weight_mine[4 * part : 4 * part + 4] = column_sum("weight", part, *weight_args[:2]).astype(bf16)
        for hops in (4, 3, 5, 2, 6, 1, 7):
            start(("weight", hops))

    def grads_step(count, carry):
        block = block_at(7 - count)
        both_groups(block, lambda part, row, slot: grads_tile(part, block, slot))

        @pl.when(count == 0)
        def _():
            last_columns("other value", *other_value)
            last_columns("own value", *own_value)
            send_dq("up", 4)
            send_dq("down", 4)

        @pl.when(count == 1)
        def _():
            send_dq("up", 3)

        @pl.when(count == 2)
        def _():
            values_summed()
            send_dq("down", 3)

        pl.when(count == 3)(lambda: send_dq("up", 2))

        @pl.when(count == 4)
        def _():
            weights_made()
            send_dq("down", 2)

        pl.when(count == 5)(lambda: send_dq("up", 1))

        @pl.when(count == 6)
        def _():
            last_columns("weight", *weight_args)
            send_dq("down", 1)

        return carry

    lax.fori_loop(0, 8, grads_step, 0)
    first_columns("other key", *other_key)
    first_columns("own key", *own_key)
    weights_summed()
    last_columns("other key", *other_key)
    last_columns("own key", *own_key)
    for part in (0, 1):
        arrived(("dq", "up", 1, part))
        arrived(("dq", "down", 1, part))
        dq_out[halves[part]] = (
            dq_acc[z, halves[part]] + dq_in[0, 0, part].astype(f32) + dq_in[1, 0, part].astype(f32)
        )
    mirrored_rows("other key", 1, other_key)
    own_rows("own key", own_key, dk_out)
    total = weight_mine[z].astype(f32)
    for hops in range(1, 8):
        arrived(("weight", hops))
        total += weight_last[hops - 1].astype(f32)
    weight_out[...] = total
    arrived(("mirror back", 1))
    dk_out[1 - group] = mirror_in[1].astype(f32)
    sender.finish()


def finish_kernel(*refs):
    sums, outs, held, load_sems, store_sems = refs[:4], refs[4:8], refs[8:12], refs[12], refs[13]
    loads = [pltpu.make_async_copy(sums[i], held[i], load_sems.at[i]) for i in range(4)]
    stores = [pltpu.make_async_copy(held[i], outs[i], store_sems.at[i]) for i in range(4)]
    for load in loads:
        load.start()
    for i in (3, 2):
        loads[i].wait()
        stores[i].start()
    for i in (0, 1):
        loads[i].wait()
        held[i][...] = 0.125 * held[i][...]
        stores[i].start()
    for store in stores:
        store.wait()


def per_device(queries, key_vectors, latents, w_value, log_sums, out_pair, cotangent, lambdas, out_gain):
    anywhere, vmem = pl.BlockSpec(memory_space=pl.ANY), pl.BlockSpec(memory_space=pltpu.VMEM)
    scratch = (
        ((8, 512, 128), bf16),
        ((8, 512, 128), bf16),
        ((8, 4, 512), f32),
        ((8, 2, 256, 256), bf16),
        ((2, 4, 256, 128), bf16),
        ((2, 4, 256, 128), bf16),
        ((9, 2, 1024, 512), bf16),
        ((256, 128), bf16),
        ((8, 256, 128), bf16),
        ((2, 512), f32),
        ((512, 256), bf16),
        ((512, 128), bf16),
        ((1, 128), f32),
        ((256, 128), bf16),
        ((8, 512, 128), f32),
        ((2, 4, 256, 128), f32),
        ((2, 4, 256, 128), f32),
        ((2, 4, 2, 256, 128), bf16),
        ((2, 4, 2, 256, 128), bf16),
        ((4, 2, 3, 128, 128), bf16),
        ((4, 2, 3, 128, 128), bf16),
        ((2, 256, 128), bf16),
        ((2, 256, 128), bf16),
        ((2, 256, 128), bf16),
        ((4, 8, 64, 128), f32),
        ((2, 3, 4, 64, 128), bf16),
        ((2, 3, 4, 64, 128), bf16),
        ((8, 64, 128), bf16),
        ((7, 64, 128), bf16),
    )
    sums = pl.pallas_call(
        whole_kernel,
        out_shape=(
            jax.ShapeDtypeStruct((512, 128), f32),
            jax.ShapeDtypeStruct((2, 256, 128), f32),
            jax.ShapeDtypeStruct((2, 256, 128), f32),
            jax.ShapeDtypeStruct((64, 128), f32),
        ),
        in_specs=[anywhere] * 8 + [pl.BlockSpec(memory_space=pltpu.SMEM)],
        out_specs=[vmem] * 4,
        scratch_shapes=[pltpu.VMEM(*entry) for entry in scratch]
        + [
            pltpu.SemaphoreType.DMA((9,)),
            pltpu.SemaphoreType.DMA((116,)),
            pltpu.SemaphoreType.DMA((116,)),
        ],
        compiler_params=pltpu.CompilerParams(
            collective_id=0, has_side_effects=True, vmem_limit_bytes=60 * 1024 * 1024
        ),
        name="whole",
    )(
        queries,
        key_vectors.reshape(2, 256, 128),
        latents.reshape(2, 256, 256),
        w_value.reshape(8, 256, 128),
        log_sums.T,
        out_pair,
        cotangent,
        out_gain.reshape(1, 128),
        lambdas,
    )
    query_grad, key_grad, value_grad, weight_grad = pl.pallas_call(
        finish_kernel,
        out_shape=tuple(jax.ShapeDtypeStruct(part.shape, f32) for part in sums),
        in_specs=[anywhere] * 4,
        out_specs=[anywhere] * 4,
        scratch_shapes=[pltpu.VMEM(part.shape, f32) for part in sums]
        + [pltpu.SemaphoreType.DMA((4,)), pltpu.SemaphoreType.DMA((4,))],
        compiler_params=pltpu.CompilerParams(vmem_limit_bytes=60 * 1024 * 1024),
        name="finish",
    )(*sums)
    return query_grad, key_grad.reshape(512, 128), value_grad.reshape(512, 128), weight_grad


def solution(mesh):
    grid = Mesh(mesh.devices.reshape(8, 4, 4, 2), ("z", "x", "y", "core"))
    sp, tp = ("z", "x"), ("y", "core")
    return jax.shard_map(
        per_device,
        mesh=grid,
        in_specs=(
            P(sp, tp),
            P(sp, tp),
            P(sp, tp),
            P(None, tp),
            P(sp, tp),
            P(sp, tp),
            P(sp, tp),
            P(tp),
            P(),
        ),
        out_specs=(P(sp, tp), P(sp, tp), P(sp, tp), P(sp, tp)),
        check_vma=False,
    )
```

time: 89.7 us -> 84.9 us (0.946)
  local copies, waits for them, and re-layouts: 3.6 us -> 0 us
  Pallas kernels: 84 us -> 82.7 us
    unnamed x8 -> x0, local copies, waits for them, and re-layouts: 3.6 us -> none
    pallas_call x1, Pallas kernels: 83.1 us -> 80.6 us  [per_device(): pl.pallas_call(whole_kernel, out_shape=(jax.ShapeDtypeStruct((512, 128),...]
    pallas_call x1, Pallas kernels: 0.93 us -> 2.06 us  [per_device(): pl.pallas_call(finish_kernel, out_shape=tuple((jax.ShapeDtypeStruct(part....]
where the time goes in v6:
time: 84.9 us; the launch traced here: 83.9 us
  Pallas kernels  82.7 us (97%)
  between operations  1.29 us (2%)
    pallas_call x1, Pallas kernels, per_device(): pl.pallas_call(whole_kernel, out_shape=(jax.ShapeDtypeStruct((512, 128),...  80.6 us
    pallas_call x1, Pallas kernels, per_device(): pl.pallas_call(finish_kernel, out_shape=tuple((jax.ShapeDtypeStruct(part....  2.06 us

profile of v6, /device:TPU:8, one launch (start us, length us, event | category | flops | bytes accessed | tf_op | source)
XLA Modules:
  0.0 83.9 jit_solution(11204147948411340870)
XLA Ops:
  1.3 80.6 %whole.1 = (f32[512,128]{1,0:T(8,128)}, f32[2,256,128]{2,1,0:T(8,128)}, f32[2,256,128]{2,1,0:T(8,128)}, f32[64,128]{1,0:T(8,128)}) custom-call(bf16[512,128]{1,0:T(8,128)(2,1)} %query_hbm.1, bf16[2,256,128]{2,1,0:T(8,128)(2,1)} %bitcast.9, bf16[2,256,256]{2,1,0:T(8,128)(2,1)} %bitcast.8, bf16[8,256,128]{2,1,0:T(8,128)(2,1)} %bitcast.7, f32[2,512]{1,0:T(2,128)} %bitcast.10, ...), custom_call_target="tpu_custom_call" | custom-call | tf_op jit(solution)/shard_map/whole/pallas_call | solution.py:564
  81.9 2.1 %finish.1 = (f32[512,128]{1,0:T(8,128)}, f32[2,256,128]{2,1,0:T(8,128)}, f32[2,256,128]{2,1,0:T(8,128)}, f32[64,128]{1,0:T(8,128)}) custom-call(f32[512,128]{1,0:T(8,128)} %get-tuple-element.12.refs_0_, f32[2,256,128]{2,1,0:T(8,128)} %get-tuple-element.13.refs_1_, f32[2,256,128]{2,1,0:T(8,128)} %get-tuple-element.14.refs_2_, f32[64,128]{1,0:T(8,128)} %get-tuple-element.15.refs_3_), custom_call_target="tpu_custom_call" | custom-call | tf_op jit(solution)/shard_map/finish/pallas_call | solution.py:595

commit v7 on v6

--- a/solution.py
+++ b/solution.py
@@ -59,9 +59,9 @@
 
 def whole_kernel(
     query_hbm, key_hbm, latent_hbm, weight_hbm, log_hbm, pair_hbm, cotangent_hbm, gain_hbm, lam_ref,
-    dq_out, dk_out, dv_out, weight_out,
+    dq_hbm, dk_hbm, dv_hbm, sum_hbm,
     query_all, grad_all, row_all, latent_all, key_all, value_all,
-    maps, key_given, weight_ref, log_ref, pair_ref, cotangent_ref, gain_ref, value_own,
+    dq_out, dk_out, dv_out, weight_out, maps, key_given, weight_ref, log_ref, pair_ref, cotangent_ref, gain_ref, value_own,
     dq_acc, dk_acc, dv_acc, dq_in, dq_stage, column_in, column_stage,
     mirror_stage, mirror_in, value_narrow,
     weight_part, weight_stage, weight_in, weight_mine, weight_last,
@@ -98,6 +98,22 @@
     sender = Sender(send_sems, recv_sems)
     plan, start, arrived = sender.plan, sender.start, sender.arrived
     halves = (pl.ds(0, 256), pl.ds(256, 256))
+
+    stores = {
+        name: pltpu.make_async_copy(source, target, local_sems.at[9 + place])
+        for place, (name, source, target) in enumerate(
+            (
+                ("dq0", dq_out.at[halves[0]], dq_hbm.at[halves[0]]),
+                ("dq1", dq_out.at[halves[1]], dq_hbm.at[halves[1]]),
+                ("dk", dk_out, dk_hbm),
+                ("dv", dv_out, dv_hbm),
+                ("weight", weight_out, sum_hbm),
+            )
+        )
+    }
+
+    def store(name):
+        stores[name].start()
 
     def latent_slot(step, toks, part=None):
         slot = latent_all.at[turned(y, step, 4) * 2 + core, toks]
@@ -254,14 +270,14 @@
     latents_far("given")
     open_latents("own")
     share_mirrored("key")
+    pass_query(0, 0)
     latents_near("given")
+    share_far("key")
     latents_last("given")
     loads["weight"].wait()
-    pass_query(0, 0)
+    latents_far("own")
     value_own[...] = values_of("given", 1 - half)
     start(("value", "mirror"))
-    share_far("key")
-    latents_far("own")
     pass_query(0, 1)
     latents_near("own")
     close_share("key")
@@ -373,17 +389,14 @@
         for part in (0, 1):
             out[group, 128 * part : 128 * part + 128] = column_sum(name, part, *args[:2])
 
-    def send_dq(way, hops):
+    def send_dq(way, hops, part):
         number, sign = (0, 1) if way == "up" else (1, -1)
-        for part in (number, 1 - number):
-            if hops == 4 and part != number:
-                continue
-            value = dq_acc[turned(z, sign * hops, 8), halves[part]]
-            if hops < 3 or (hops == 3 and part == number):
-                arrived(("dq", way, hops + 1, part))
-                value += dq_in[number, hops, part].astype(f32)
-            dq_stage[number, hops - 1, part] = value.astype(bf16)
-            start(("dq", way, hops, part))
+        value = dq_acc[turned(z, sign * hops, 8), halves[part]]
+        if hops < 3 or (hops == 3 and part == number):
+            arrived(("dq", way, hops + 1, part))
+            value += dq_in[number, hops, part].astype(f32)
+        dq_stage[number, hops - 1, part] = value.astype(bf16)
+        start(("dq", way, hops, part))
 
     def maps_step(count, carry):
         @pl.when(count == 1)
@@ -421,13 +434,7 @@
 
     lax.fori_loop(0, 8, maps_step, 0)
     first_columns("other value", *other_value)
-    first_columns("own value", *own_value)
     close_share("value")
-
-    def values_summed():
-        mirrored_rows("other value", 0, other_value)
-        own_rows("own value", own_value, dv_out)
-        value_narrow[group] = dv_out[group].astype(bf16)
 
     def weights_made():
         arrived(("mirror back", 0))
@@ -451,63 +458,88 @@
         for hops in (4, 3, 5, 2, 6, 1, 7):
             start(("weight", hops))
 
+    def tile_at(count):
+        found, passed = jnp.int32(0), jnp.int32(0)
+        for row in (7 - z, z):
+            for hops in (4, 3, 5, 2, 6, 1, 7, 0):
+                block = turned(z, hops, 8)
+                counts = block >= row
+                found = jnp.where(counts & (passed == count), block, found)
+                passed = passed + jnp.where(counts, 1, 0)
+        return found
+
     def grads_step(count, carry):
-        block = block_at(7 - count)
-        both_groups(block, lambda part, row, slot: grads_tile(part, block, slot))
-
-        @pl.when(count == 0)
+        other = count <= z
+        block = tile_at(count)
+        part = jnp.where(other, 1 - group, group)
+        grads_tile(part, block, jnp.where(other, block - 7 + z, block + 1))
+
+        @pl.when(count == 1)
         def _():
             last_columns("other value", *other_value)
+            first_columns("own value", *own_value)
+
+        @pl.when(count == 3)
+        def _():
+            mirrored_rows("other value", 0, other_value)
             last_columns("own value", *own_value)
-            send_dq("up", 4)
-            send_dq("down", 4)
-
-        @pl.when(count == 1)
-        def _():
-            send_dq("up", 3)
-
-        @pl.when(count == 2)
-        def _():
-            values_summed()
-            send_dq("down", 3)
-
-        pl.when(count == 3)(lambda: send_dq("up", 2))
-
-        @pl.when(count == 4)
-        def _():
-            weights_made()
-            send_dq("down", 2)
-
-        pl.when(count == 5)(lambda: send_dq("up", 1))
-
-        @pl.when(count == 6)
-        def _():
-            last_columns("weight", *weight_args)
-            send_dq("down", 1)
-
+
+        @pl.when(count == 5)
+        def _():
+            send_dq("up", 4, 0)
+            send_dq("down", 4, 1)
+            send_dq("up", 3, 1)
+            send_dq("down", 3, 0)
+            own_rows("own value", own_value, dv_out)
+            value_narrow[group] = dv_out[group].astype(bf16)
+
+        pl.when(count == 6)(weights_made)
+
+        @pl.when(count == 7)
+        def _():
+            send_dq("up", 3, 0)
+            send_dq("down", 3, 1)
+            send_dq("up", 2, 1)
+            send_dq("down", 2, 0)
+
+        pl.when(count == z)(lambda: first_columns("other key", *other_key))
+        pl.when((count == z + 2) & (z < 6))(lambda: last_columns("other key", *other_key))
+        pl.when((count == z + 4) & (z < 4))(lambda: mirrored_rows("other key", 1, other_key))
         return carry
 
-    lax.fori_loop(0, 8, grads_step, 0)
-    first_columns("other key", *other_key)
+    lax.fori_loop(0, 9, grads_step, 0)
     first_columns("own key", *own_key)
+    store("dv")
+    pl.when(z >= 6)(lambda: last_columns("other key", *other_key))
+    last_columns("weight", *weight_args)
+    send_dq("up", 2, 0)
+    send_dq("down", 2, 1)
+    send_dq("up", 1, 1)
+    send_dq("down", 1, 0)
+    last_columns("own key", *own_key)
+    pl.when(z >= 4)(lambda: mirrored_rows("other key", 1, other_key))
     weights_summed()
-    last_columns("other key", *other_key)
-    last_columns("own key", *own_key)
+    send_dq("up", 1, 0)
+    send_dq("down", 1, 1)
+    own_rows("own key", own_key, dk_out)
+    arrived(("mirror back", 1))
+    dk_out[1 - group] = mirror_in[1].astype(f32)
+    store("dk")
     for part in (0, 1):
         arrived(("dq", "up", 1, part))
         arrived(("dq", "down", 1, part))
         dq_out[halves[part]] = (
             dq_acc[z, halves[part]] + dq_in[0, 0, part].astype(f32) + dq_in[1, 0, part].astype(f32)
         )
-    mirrored_rows("other key", 1, other_key)
-    own_rows("own key", own_key, dk_out)
+        store("dq" + str(part))
     total = weight_mine[z].astype(f32)
     for hops in range(1, 8):
         arrived(("weight", hops))
         total += weight_last[hops - 1].astype(f32)
     weight_out[...] = total
-    arrived(("mirror back", 1))
-    dk_out[1 - group] = mirror_in[1].astype(f32)
+    store("weight")
+    for copy in stores.values():
+        copy.wait()
     sender.finish()
 
 
@@ -529,7 +561,7 @@
 
 
 def per_device(queries, key_vectors, latents, w_value, log_sums, out_pair, cotangent, lambdas, out_gain):
-    anywhere, vmem = pl.BlockSpec(memory_space=pl.ANY), pl.BlockSpec(memory_space=pltpu.VMEM)
+    anywhere = pl.BlockSpec(memory_space=pl.ANY)
     scratch = (
         ((8, 512, 128), bf16),
         ((8, 512, 128), bf16),
@@ -537,6 +569,10 @@
         ((8, 2, 256, 256), bf16),
         ((2, 4, 256, 128), bf16),
         ((2, 4, 256, 128), bf16),
+        ((512, 128), f32),
+        ((2, 256, 128), f32),
+        ((2, 256, 128), f32),
+        ((64, 128), f32),
         ((9, 2, 1024, 512), bf16),
         ((256, 128), bf16),
         ((8, 256, 128), bf16),
@@ -570,10 +606,10 @@
             jax.ShapeDtypeStruct((64, 128), f32),
         ),
         in_specs=[anywhere] * 8 + [pl.BlockSpec(memory_space=pltpu.SMEM)],
-        out_specs=[vmem] * 4,
+        out_specs=[anywhere] * 4,
         scratch_shapes=[pltpu.VMEM(*entry) for entry in scratch]
         + [
-            pltpu.SemaphoreType.DMA((9,)),
+            pltpu.SemaphoreType.DMA((14,)),
             pltpu.SemaphoreType.DMA((116,)),
             pltpu.SemaphoreType.DMA((116,)),
         ],

time: 84.9 us -> 78 us (0.919)
  Pallas kernels: 82.7 us -> 76.4 us
    pallas_call x1, Pallas kernels: 80.6 us -> 74.3 us  [per_device(): pl.pallas_call(whole_kernel, out_shape=(jax.ShapeDtypeStruct((512, 128),...]
where the time goes in v7:
time: 78 us; the launch traced here: 77.7 us
  Pallas kernels  76.4 us (98%)
  between operations  1.29 us (2%)
    pallas_call x1, Pallas kernels, per_device(): pl.pallas_call(whole_kernel, out_shape=(jax.ShapeDtypeStruct((512, 128),...  74.3 us
    pallas_call x1, Pallas kernels, per_device(): pl.pallas_call(finish_kernel, out_shape=tuple((jax.ShapeDtypeStruct(part....  2.06 us

profile of v7, /device:TPU:8, one launch (start us, length us, event | category | flops | bytes accessed | tf_op | source)
XLA Modules:
  0.0 77.7 jit_solution(11388149346307123742)
XLA Ops:
  1.3 74.3 %whole.1 = (f32[512,128]{1,0:T(8,128)}, f32[2,256,128]{2,1,0:T(8,128)}, f32[2,256,128]{2,1,0:T(8,128)}, f32[64,128]{1,0:T(8,128)}) custom-call(bf16[512,128]{1,0:T(8,128)(2,1)} %query_hbm.1, bf16[2,256,128]{2,1,0:T(8,128)(2,1)} %bitcast.9, bf16[2,256,256]{2,1,0:T(8,128)(2,1)} %bitcast.8, bf16[8,256,128]{2,1,0:T(8,128)(2,1)} %bitcast.7, f32[2,512]{1,0:T(2,128)} %bitcast.10, ...), custom_call_target="tpu_custom_call" | custom-call | tf_op jit(solution)/shard_map/whole/pallas_call | solution.py:600
  75.6 2.1 %finish.1 = (f32[512,128]{1,0:T(8,128)}, f32[2,256,128]{2,1,0:T(8,128)}, f32[2,256,128]{2,1,0:T(8,128)}, f32[64,128]{1,0:T(8,128)}) custom-call(f32[512,128]{1,0:T(8,128)} %get-tuple-element.12.refs_0_, f32[2,256,128]{2,1,0:T(8,128)} %get-tuple-element.13.refs_1_, f32[2,256,128]{2,1,0:T(8,128)} %get-tuple-element.14.refs_2_, f32[64,128]{1,0:T(8,128)} %get-tuple-element.15.refs_3_), custom_call_target="tpu_custom_call" | custom-call | tf_op jit(solution)/shard_map/finish/pallas_call | solution.py:631

commit v8 on v7

--- a/solution.py
+++ b/solution.py
@@ -16,7 +16,7 @@
 rows_by_cols = (((1,), (0,)), ((), ()))
 cols_by_cols = (((0,), (0,)), ((), ()))
 mesh_ids = pl.DeviceIdType.MESH
-tok_len = 256
+tok_len = 512
 
 
 class Sender:

time: 78 us -> 77.4 us (level)
  no operation moved by 1% of the time
where the time goes in v8:
time: 77.4 us; the launch traced here: 77.3 us
  Pallas kernels  76 us (98%)
  between operations  1.29 us (2%)
    pallas_call x1, Pallas kernels, per_device(): pl.pallas_call(whole_kernel, out_shape=(jax.ShapeDtypeStruct((512, 128),...  73.9 us
    pallas_call x1, Pallas kernels, per_device(): pl.pallas_call(finish_kernel, out_shape=tuple((jax.ShapeDtypeStruct(part....  2.06 us

profile of v8, /device:TPU:8, one launch (start us, length us, event | category | flops | bytes accessed | tf_op | source)
XLA Modules:
  0.0 77.3 jit_solution(3905149996216877532)
XLA Ops:
  1.3 73.9 %whole.1 = (f32[512,128]{1,0:T(8,128)}, f32[2,256,128]{2,1,0:T(8,128)}, f32[2,256,128]{2,1,0:T(8,128)}, f32[64,128]{1,0:T(8,128)}) custom-call(bf16[512,128]{1,0:T(8,128)(2,1)} %query_hbm.1, bf16[2,256,128]{2,1,0:T(8,128)(2,1)} %bitcast.9, bf16[2,256,256]{2,1,0:T(8,128)(2,1)} %bitcast.8, bf16[8,256,128]{2,1,0:T(8,128)(2,1)} %bitcast.7, f32[2,512]{1,0:T(2,128)} %bitcast.10, ...), custom_call_target="tpu_custom_call" | custom-call | tf_op jit(solution)/shard_map/whole/pallas_call | solution.py:600
  75.2 2.1 %finish.1 = (f32[512,128]{1,0:T(8,128)}, f32[2,256,128]{2,1,0:T(8,128)}, f32[2,256,128]{2,1,0:T(8,128)}, f32[64,128]{1,0:T(8,128)}) custom-call(f32[512,128]{1,0:T(8,128)} %get-tuple-element.12.refs_0_, f32[2,256,128]{2,1,0:T(8,128)} %get-tuple-element.13.refs_1_, f32[2,256,128]{2,1,0:T(8,128)} %get-tuple-element.14.refs_2_, f32[64,128]{1,0:T(8,128)} %get-tuple-element.15.refs_3_), custom_call_target="tpu_custom_call" | custom-call | tf_op jit(solution)/shard_map/finish/pallas_call | solution.py:631
